TPU v7x, 512 devices: a whole 4x4x16 slice. The times are simulated.
512 devices in a mesh: sp: 32 (over z, core), tp: 16 (over y, x).
Axes of the slice: x: 4, y: 4, z: 16, core: 2. Of those that a mesh axis runs over, the one named last changes fastest.
Arguments:
- layer_input: bfloat16 [8, 4096, 2048], P(None, 'sp', 'tp'), may hold values from -6 to 6
- w_key: bfloat16 [2048, 2048], P(None, 'tp'), may hold values from -0.125 to 0.125
- w_value: bfloat16 [2048, 2048], P(None, 'tp'), may hold values from -0.125 to 0.125
- w_gates: bfloat16 [2, 2048, 16], replicated, may hold values from -0.125 to 0.125
- decay_rate: float32 [16], P('tp'), may hold values from 0 to 1, as said below
- beta_bias: float32 [16], P('tp'), may hold values from -5.5 to -3
- log_decay_extra: float32 [8, 16, 4096], P(None, 'tp', 'sp'), may hold values from -2 to 0, as said below
- new_query: bfloat16 [8, 2048], P(None, 'tp'), may hold values from -6 to 6
- read_gain: float32 [128], replicated, may hold values from 0.1 to 1.9
Outputs:
- state_cache: bfloat16 [1024, 2048], P('sp', 'tp')
- first_read: bfloat16 [8, 2048], P(None, 'tp')
Inputs may be any that keep to these rules, and one draw needn't show every extreme that they name: `decay_rate`: a positive rate for each head. `log_decay_extra`: additions that are never positive.
All inputs are finite; a program needn't handle non-finite values.
Results may differ from a plain program's by a relative error of at most 0.0052.
Values may be sent and summed in bfloat16 or wider, within the bound.
No kernel may reach another device: no remote copies, remote signals or barrier semaphores. Data moves between devices by JAX's collectives and lax.ppermute only.
A program may use at most 64 MiB of HBM per device.

v0:
```python
import jax
import jax.numpy as jnp
from jax import lax
from jax.sharding import Mesh
from jax.sharding import PartitionSpec as P

DK = 128
DV = 128
BLOCK = 64
SP = ("sp_0", "sp_1")


EPS = 1e-06
HIGH = lax.Precision.HIGHEST


def nothing_yet(x, identity):
    return jnp.broadcast_to(jnp.asarray(identity, x.dtype), x.shape)


def prefix_by_axis(x, axes, combine, identity):
    before = start = nothing_yet(x, identity)
    total = x
    for axis in reversed(axes):
        count, position = (lax.axis_size(axis), lax.axis_index(axis))
        pieces = lax.all_gather(total, axis)
        inside, total = (start, start)
        for k in reversed(range(count)):
            passed = k > position
            total = combine(total, pieces[k])
            inside = jnp.where(passed, total, inside)
        before = combine(inside, before)
    return before


def cut_along(x, dim, count):
    shape = x.shape
    pieces = x.reshape(*shape[:dim], count, shape[dim] // count, *shape[dim + 1 :])
    return jnp.moveaxis(pieces, dim, 0)


def summed_on_arrival(x, axis, dim):
    pieces = cut_along(x, dim, lax.axis_size(axis))
    arrived = lax.all_to_all(pieces, axis, split_axis=0, concat_axis=0, tiled=True)
    return arrived.sum(axis=0)


def sent_to_all(x, axis):
    count = lax.axis_size(axis)
    return lax.all_to_all(jnp.broadcast_to(x[None], (count, *x.shape)), axis, 0, 0, tiled=True)


def taken_together(x, axis):
    return sent_to_all(x, axis).sum(axis=0)


def unit_rows(values):
    return values * lax.rsqrt(jnp.sum(values * values, axis=-1, keepdims=True) + EPS)


def matmul_high(left, right):
    return jnp.einsum("...ab,...bc->...ac", left, right, precision=HIGH)


def block_pieces(keys, values, log_decay, beta):
    size = keys.shape[-2]
    width = values.shape[-1]
    running = jnp.cumsum(log_decay, axis=-1)
    sequence_indices = jnp.arange(size)
    causal = sequence_indices[:, None] >= sequence_indices[None, :]
    strict = sequence_indices[:, None] > sequence_indices[None, :]
    spread = running[..., :, None] - running[..., None, :]
    weights = jnp.where(causal, jnp.exp(jnp.where(causal, spread, 0.0)), 0.0)
    key_beta = keys * beta[..., None]
    lower = jnp.where(
        strict, jnp.einsum("...cd,...sd->...cs", key_beta, keys, precision=HIGH) * weights, 0.0
    )
    right_side = jnp.concatenate(
        [values * beta[..., None], key_beta * jnp.exp(running)[..., None]], axis=-1
    )
    solved = lax.linalg.triangular_solve(
        lower, right_side, left_side=True, lower=True, unit_diagonal=True
    )
    fresh = solved[..., :width]
    erase = solved[..., width:]
    last = running[..., -1]
    key_late = keys * jnp.exp(last[..., None] - running)[..., None]
    identity = jnp.eye(keys.shape[-1], dtype=jnp.float32)
    transition = jnp.exp(last)[..., None, None] * identity - jnp.einsum(
        "...cd,...ce->...de", key_late, erase, precision=HIGH
    )
    inject = jnp.einsum("...cd,...cv->...dv", key_late, fresh, precision=HIGH)
    return (transition, inject)


def shards(
    layer_input,
    w_key,
    w_value,
    w_gates,
    decay_rate,
    beta_bias,
    log_decay_extra,
    new_query,
    read_gain,
):
    prompts, seg_len, _ = layer_input.shape
    heads_here = w_key.shape[1] // DK
    blocks = seg_len // BLOCK
    first_head = lax.axis_index("tp") * heads_here
    gate_cols = lax.dynamic_slice_in_dim(w_gates, first_head, heads_here, 2)
    joined = jnp.concatenate([w_key, w_value], axis=1)
    piece = lax.all_gather(layer_input, "tp", axis=2, tiled=True)
    pair_sum = jnp.einsum("std,de->ste", piece, joined, preferred_element_type=jnp.float32)
    gate_sum = jnp.einsum("std,gdh->gsth", piece, gate_cols, preferred_element_type=jnp.float32)
    key_pre = pair_sum[..., : heads_here * DK].reshape(prompts, seg_len, heads_here, DK)
    value_pre = pair_sum[..., heads_here * DK :].reshape(prompts, seg_len, heads_here, DV)
    keys = unit_rows(jax.nn.silu(key_pre))
    values = jax.nn.silu(value_pre)
    log_decay = -decay_rate * jax.nn.softplus(gate_sum[0]) + log_decay_extra.transpose(0, 2, 1)
    beta = jax.nn.sigmoid(gate_sum[1] + beta_bias)
    key_blocks = keys.reshape(prompts, blocks, BLOCK, heads_here, DK).transpose(0, 3, 1, 2, 4)
    value_tiles = values.reshape(prompts, blocks, BLOCK, heads_here, DV).transpose(0, 3, 1, 2, 4)
    decay_blocks = log_decay.reshape(prompts, blocks, BLOCK, heads_here).transpose(0, 3, 1, 2)
    strength_groups = beta.reshape(prompts, blocks, BLOCK, heads_here).transpose(0, 3, 1, 2)
    transition, inject = block_pieces(key_blocks, value_tiles, decay_blocks, strength_groups)

    def compose_maps(carry, piece):
        total_map, total_add = carry
        block_map, block_add = piece
        return (
            (matmul_high(block_map, total_map), matmul_high(block_map, total_add) + block_add),
            None,
        )

    identity = jnp.eye(DK, dtype=jnp.float32)
    map_start = jnp.broadcast_to(identity, (prompts, heads_here, DK, DK))
    add_start = jnp.zeros((prompts, heads_here, DK, DV), jnp.float32)
    (seg_map, seg_add), _ = lax.scan(
        compose_maps,
        (map_start, add_start),
        (jnp.moveaxis(transition, 2, 0), jnp.moveaxis(inject, 2, 0)),
    )
    local_rows = prompts * DK // lax.axis_size(SP)
    leading_line = lax.axis_index(SP) * local_rows
    query = new_query.reshape(prompts, heads_here, DK)

    def later_first(earlier, later):
        return matmul_high(earlier, later)

    after = prefix_by_axis(seg_map, SP, later_first, map_start)
    term = jnp.einsum("shab,shbv->sahv", after, seg_add, precision=HIGH).reshape(
        prompts * DK, heads_here * DV
    )
    owned = summed_on_arrival(term, SP, 0)
    state_cache = owned.astype(jnp.bfloat16)
    query_rows = query.transpose(0, 2, 1).reshape(prompts * DK, heads_here)
    my_query = lax.dynamic_slice_in_dim(query_rows, leading_line, local_rows, 0)
    owner = (leading_line + jnp.arange(local_rows)) // DK
    member = (owner[:, None] == jnp.arange(prompts)[None, :]).astype(jnp.float32)
    weighted = my_query.astype(jnp.float32)[:, :, None] * state_cache.reshape(
        local_rows, heads_here, DV
    ).astype(jnp.float32)
    partial_read = jnp.einsum("rs,rhv->shv", member, weighted, precision=HIGH)
    raw_read = taken_together(partial_read, SP)
    scaled = (
        raw_read
        * lax.rsqrt(jnp.mean(raw_read * raw_read, axis=-1, keepdims=True) + EPS)
        * read_gain
    )
    first_read = scaled.astype(jnp.bfloat16).reshape(prompts, heads_here * DV)
    return (state_cache, first_read)


def solution(mesh):
    finer = Mesh(mesh.devices.reshape(16, 2, mesh.shape["tp"]), ("sp_0", "sp_1", "tp"))
    placed = (
        P(None, SP, "tp"),
        P(None, "tp"),
        P(None, "tp"),
        P(),
        P("tp"),
        P("tp"),
        P(None, "tp", SP),
        P(None, "tp"),
        P(),
    )
    return jax.shard_map(
        shards, mesh=finer, in_specs=placed, out_specs=(P(SP, "tp"), P(None, "tp")), check_vma=False
    )
```

profile of v0, /device:TPU:1, one launch (start us, length us, event | category | flops | bytes accessed | tf_op | source)
XLA Modules:
  0.0 407.0 jit_solution(17985307926556200827)
XLA Ops:
  9.8 1.4 reduce.14
  11.5 75.6 %all-gather.6.cloned.1.call-done = bf16[8,128,2048]{2,1,0:T(8,128)(2,1)} async-done(((bf16[8,128,128]{2,1,0:T(8,128)(2,1)}), bf16[8,128,2048]{2,1,0:T(8,128)(2,1)}) %all-gather.6.cloned.1.call-update) | async-done | bytes 4194320 | tf_op jit(solution)/shard_map/all_gather | solution.py:113
  87.1 3.4 fusion.75
  91.4 3.8 convolution_bitcast_fusion.2
  95.8 1.1 fusion.13
  96.9 78.6 %custom-call.3 = f32[8,1,2,1,64,64]{4,5,3,2,1,0:T(8,128)S(1)} custom-call(f32[8,1,2,1,64,64]{5,4,3,2,1,0:T(8,128)S(1)} %fusion.13), custom_call_target="InvertDiagBlocksLowerTriangular" | custom-call | tf_op jit(solution)/shard_map/triangular_solve | solution.py:81
  176.9 2.0 convolution_bitcast_fusion.1
  178.9 2.0 fusion.9
  181.0 2.8 while.12
  184.9 21.7 %all-gather.8.cloned.1.call-done = f32[16,1,128,128]{3,2,1,0:T(8,128)} async-done(((f32[8,1,128,128]{3,2,1,0:T(8,128)}), f32[16,1,128,128]{3,2,1,0:T(8,128)}) %all-gather.8.cloned.1.call-update) | async-done | bytes 1048592 | tf_op jit(solution)/shard_map/all_gather | solution.py:26
  206.6 1.6 fusion.51
  208.3 2.5 fusion.50
  211.5 105.1 %all-gather.10.cloned.1.call-done = f32[128,128,128]{2,1,0:T(8,128)} async-done(((f32[8,128,128]{2,1,0:T(8,128)}), f32[128,128,128]{2,1,0:T(8,128)}) %all-gather.10.cloned.1.call-update) | async-done | bytes 8388624 | tf_op jit(solution)/shard_map/all_gather | solution.py:26
  316.6 1.8 fusion.48
  318.3 2.1 fusion.46
  320.5 1.7 fusion.44
  322.2 1.7 fusion.42
  323.9 1.7 fusion.40
  325.6 1.7 fusion.38
  333.3 1.3 convolution_select_fusion
  335.2 1.4 fusion.52
  336.7 9.8 %all-to-all-start = ((f32[32,32,128]{2,1,0:T(8,128)}), f32[32,32,128]{2,1,0:T(8,128)S(1)}, u32[]{:S(2)}, u32[]{:S(2)}) async-start(f32[32,32,128]{2,1,0:T(8,128)} %bitcast.32), calls=%async_computation | async-start | bytes 1048576 | tf_op jit(solution)/shard_map/all_to_all | solution.py:44
  346.6 33.4 %all-to-all-done = f32[32,32,128]{2,1,0:T(8,128)S(1)} async-done(((f32[32,32,128]{2,1,0:T(8,128)}), f32[32,32,128]{2,1,0:T(8,128)S(1)}, u32[]{:S(2)}, u32[]{:S(2)}) %all-to-all-start) | async-done | bytes 524320 | tf_op jit(solution)/shard_map/all_to_all | solution.py:44
  380.3 19.3 %all_to_all.10 = f32[32,8,1,128]{3,1,2,0:T(8,128)S(1)} all-to-all(f32[32,8,1,128]{3,1,2,0:T(8,128)S(1)} %broadcast_in_dim.27), channel_id=1, replica_groups=mesh['sp_0'=16,'sp_1'=2,'tp'=16] {'sp_0','sp_1'}, dimensions={0} | all-to-all | bytes 262144 | tf_op jit(solution)/shard_map/all_to_all | solution.py:50
  (74 shorter events, 16.8 us)
Async XLA Ops:
  7.2 4.2 %copy-start = (bf16[2,2048,16]{1,2,0:T(8,128)(2,1)S(1)}, bf16[2,2048,16]{1,2,0:T(8,128)(2,1)}, u32[]{:S(2)}) copy-start(bf16[2,2048,16]{1,2,0:T(8,128)(2,1)} %param.14) | copy-start | bytes 393220
  7.2 79.9 %all-gather.6.cloned.1.call-start = ((), (), s32[]{:S(2)}) async-start(), calls=%async_computation.2 | async-start | bytes 4456448 | tf_op jit(solution)/shard_map/all_gather | solution.py:113
  7.9 198.7 %all-gather.8.cloned.1.call-start = ((), (), s32[]{:S(2)}) async-start(), calls=%async_computation.3 | async-start | bytes 1572864 | tf_op jit(solution)/shard_map/all_gather | solution.py:26
  183.9 0.8 copy-start.1
  184.7 131.9 %all-gather.10.cloned.1.call-start = ((), (), s32[]{:S(2)}) async-start(), calls=%async_computation.4 | async-start | bytes 8912896 | tf_op jit(solution)/shard_map/all_gather | solution.py:26
  316.6 10.7 %copy-start.2 = (f32[128,128,128]{2,1,0:T(8,128)S(1)}, f32[128,128,128]{2,1,0:T(8,128)}, u32[]{:S(2)}) copy-start(f32[128,128,128]{2,1,0:T(8,128)} %all-gather.10.cloned.1.call-done) | copy-start | bytes 25165828
  331.9 14.5 %copy-start.4 = (bf16[8,128]{1,0:T(8,128)(2,1)S(1)}, bf16[8,128]{1,0:T(8,128)(2,1)}, u32[]{:S(2)}) copy-start(bf16[8,128]{1,0:T(8,128)(2,1)} %param.18) | copy-start | bytes 6148
  331.9 67.8 %copy-start.5 = (f32[128]{0:T(128)S(1)}, f32[128]{0:T(128)}, u32[]{:S(2)}) copy-start(f32[128]{0:T(128)} %param.19) | copy-start | bytes 1540
  336.7 43.3 %all-to-all-start = ((f32[32,32,128]{2,1,0:T(8,128)}), f32[32,32,128]{2,1,0:T(8,128)S(1)}, u32[]{:S(2)}, u32[]{:S(2)}) async-start(f32[32,32,128]{2,1,0:T(8,128)} %bitcast.32), calls=%async_computation | async-start | bytes 1048576 | tf_op jit(solution)/shard_map/all_to_all | solution.py:44
  380.0 20.4 %copy-start.3 = (bf16[32,128]{1,0:T(8,128)(2,1)}, bf16[32,128]{1,0:T(8,128)(2,1)S(1)}, u32[]{:S(2)}) copy-start(bf16[32,128]{1,0:T(8,128)(2,1)S(1)} %reduce_sum.37) | copy-start | bytes 24580
Sparse Core Ops, SparseCore 0:
  11.0 76.0 all-gather.5
  184.8 21.7 all-gather.7
  210.9 105.5 all-gather.9
where the time goes:
time: 408 us; the launch traced here: 407 us
  waiting for transfers between devices  236 us (58%)
  other arithmetic  82.5 us (20%)
  matrix products  40.8 us (10%)
  blocking collectives  19.3 us (5%)
  between operations  15.5 us (4%)
  starting transfers between devices  10.1 us (2%)
    all_gather x2, waiting for transfers between devices, prefix_by_axis(): pieces = lax.all_gather(total, axis)  127 us
    another operation x3, other arithmetic, block_pieces(): lax.linalg.triangular_solve(lower, right_side, left_side=True, lower=True...  78.7 us
    all_gather x1, waiting for transfers between devices, shards(): piece = lax.all_gather(layer_input, 'tp', axis=2, tiled=True)  75.6 us
    all_to_all x1, waiting for transfers between devices, summed_on_arrival(): lax.all_to_all(pieces, axis, split_axis=0, concat_axis=0, tiled=True)  33.4 us
    dot_general x24, matrix products, matmul_high(): return jnp.einsum('...ab,...bc->...ac', left, right, precision=HIGH)  25.9 us
    all_to_all x1, blocking collectives, sent_to_all(): lax.all_to_all(jnp.broadcast_to(x[None], (count, *x.shape)), axis, 0, 0,...  19.3 us
    all_to_all x1, starting transfers between devices, summed_on_arrival(): lax.all_to_all(pieces, axis, split_axis=0, concat_axis=0, tiled=True)  9.76 us
  transfers between devices with their start and end apart: 4, of which 4 were waited for; matrix products, arithmetic and copies ran while one was open for 1% of the time, Pallas kernels for 0%

commit v1 on v0

v1 whole, which is shorter than its diff:
```python
import jax
import jax.numpy as jnp
from jax import lax
from jax.experimental import pallas as pl
from jax.experimental.pallas import tpu as pltpu
from jax.sharding import PartitionSpec as P


DK = 128
DV = 128
BLOCK = 128
EPS = 1e-06
HIGH = lax.Precision.HIGHEST
F32 = jnp.float32
BF16 = jnp.bfloat16
PAD = 16


MIB = 1 << 20
VMEM = pl.BlockSpec(memory_space=pltpu.VMEM)
SMEM = pl.BlockSpec(memory_space=pltpu.SMEM)


def granted(mib):
    return pltpu.CompilerParams(vmem_limit_bytes=mib * MIB)


NN = (((1,), (0,)), ((), ()))
NT = (((1,), (1,)), ((), ()))


def dot1(left, right, dims=NN):
    return lax.dot_general(left, right, dims, preferred_element_type=F32)


def halves(x):
    high = x.astype(BF16)
    low = (x - high.astype(F32)).astype(BF16)
    return high, low


def dot3(left, right, dims=NN):
    lh, ll = left if isinstance(left, tuple) else halves(left)
    rh, rl = right if isinstance(right, tuple) else halves(right)
    return dot1(lh, rh, dims) + (dot1(ll, rh, dims) + dot1(lh, rl, dims))


def unit_lower_inverse(low, row, col):
    size = low.shape[0]
    eye = (row == col).astype(F32)
    step = 1
    inverse = eye
    while step < size:
        merge = ((row // (2 * step)) == (col // (2 * step))) & ((row // step) != (col // step))
        part = jnp.where(merge, low, 0.0)
        if step == 1:
            inverse = eye - part
        else:
            held = inverse.astype(BF16)
            inverse = inverse - dot1(dot1(held, part.astype(BF16)).astype(BF16), held)
        step *= 2
    return inverse


def three_pieces(x):
    high = x.astype(BF16).astype(F32)
    rest = x - high
    mid = rest.astype(BF16).astype(F32)
    return high, mid, (rest - mid).astype(BF16).astype(F32)


def pack_kernel(x, extra, out):
    prompts, seg, width = x.shape
    out[:, :seg, :] = x[...]
    pieces = three_pieces(extra[...])
    for p in range(prompts):
        rows = [piece[p : p + 1] for piece in pieces] + [jnp.zeros((PAD - 3, width), F32)]
        out[p, seg:, :] = jnp.concatenate(rows, axis=0).astype(BF16)


def packed(layer_input, extra):
    prompts, seg, width = layer_input.shape
    return pl.pallas_call(
        pack_kernel,
        in_specs=[VMEM, VMEM],
        out_specs=VMEM,
        out_shape=jax.ShapeDtypeStruct((prompts, seg + PAD, width), BF16),
        compiler_params=granted(4),
    )(layer_input, extra)


def parcel_kernel(here, rate, bias, out):
    segs, rows, width = here.shape
    seg = rows - PAD
    half = segs // 2
    lane = lax.broadcasted_iota(jnp.int32, (1, width), 1)
    consts = three_pieces(jnp.where(lane < width // 2, rate[0], bias[0]))
    for which in range(2):
        tails = [here[half * which + b, seg:, :].astype(F32) for b in range(half)]
        tail = [tails[b][i : i + 1] for i in range(3) for b in range(half)]
        tail = jnp.concatenate(tail + list(consts) + [jnp.zeros((PAD - 3 * half - 3, width), F32)], axis=0)
        tail = tail.astype(BF16)
        body = [here[half * which + b, :seg, :] for b in range(half)]
        for other in range(which, out.shape[0], 2):
            for b in range(half):
                out[other, seg * b : seg * (b + 1), :] = body[b]
            out[other, seg * half :, :] = tail


def parcels(here, rate, bias, count):
    segs, rows, width = here.shape
    return pl.pallas_call(
        parcel_kernel,
        in_specs=[VMEM, SMEM, SMEM],
        out_specs=VMEM,
        out_shape=jax.ShapeDtypeStruct((count, (segs // 2) * (rows - PAD) + PAD, width), BF16),
        compiler_params=granted(8),
    )(here, rate, bias)


def map_kernel(xg, wk, wv, wo, wg, mine, other, acc, gates):
    sources, rows, width = xg.shape
    rows = rows - PAD
    blocks = rows // BLOCK
    me = lax.axis_index("tp")
    x = jnp.concatenate([xg[i, :rows, :] for i in range(sources)], axis=1)
    acc[0] = dot1(x, jnp.concatenate([wk[...], wv[...]], axis=1))
    acc[1] = dot1(x, jnp.concatenate([wo[0], wo[1]], axis=1))
    gates[...] = dot1(wg[...], x, NT)

    row = lax.broadcasted_iota(jnp.int32, (BLOCK, BLOCK), 0)
    col = lax.broadcasted_iota(jnp.int32, (BLOCK, BLOCK), 1)
    upto = (row <= col).astype(F32)
    decays, betas = [], []
    for which in range(2):
        head = me if which == 0 else me ^ 1
        extras = xg[head, rows:, :].astype(F32)
        extra = extras[0:4] + extras[4:8] + extras[8:12]
        consts = extras[12:13] + extras[13:14] + extras[14:15]
        rate, bias = consts[:, 0:1], consts[:, width // 2 : width // 2 + 1]
        cut = lambda g: jnp.concatenate(
            [g[:, BLOCK * b : BLOCK * (b + 1)] for b in range(blocks)], axis=0
        )
        decay_pre = cut(gates[pl.ds(head, 1), :])
        beta_pre = cut(gates[pl.ds(sources + head, 1), :])
        soft = jnp.maximum(decay_pre, 0.0) + jnp.log1p(jnp.exp(-jnp.abs(decay_pre)))
        decays.append(-rate * soft + extra)
        betas.append(jax.nn.sigmoid(beta_pre + bias))
    running = jnp.dot(
        jnp.concatenate(decays, axis=0), upto, precision=HIGH, preferred_element_type=F32
    )
    beta = jnp.concatenate(betas, axis=0)
    units = 2 * blocks
    tall = jnp.concatenate([running, beta, jnp.zeros((BLOCK - 2 * units, BLOCK), F32)], axis=0)
    columns = tall.T
    for which in range(2):
        maps = []
        for b in range(blocks):
            u = which * blocks + b
            pre = acc[which, BLOCK * b : BLOCK * (b + 1), :]
            act = pre * jax.nn.sigmoid(pre)
            key, value = act[:, :DK], act[:, DK:]
            key = key * lax.rsqrt(jnp.sum(key * key, axis=1, keepdims=True) + EPS)
            run_row = jnp.broadcast_to(running[u : u + 1, :], (BLOCK, BLOCK))
            run_col = jnp.broadcast_to(columns[:, u : u + 1], (BLOCK, BLOCK))
            beta_col = jnp.broadcast_to(columns[:, units + u : units + u + 1], (BLOCK, BLOCK))
            last = jnp.broadcast_to(running[u : u + 1, BLOCK - 1 :], (BLOCK, BLOCK))
            split = halves(key)
            gram = dot3(split, split, NT)
            strict = row > col
            weights = jnp.exp(jnp.where(strict, run_col - run_row, 0.0))
            low = jnp.where(strict, gram * beta_col * weights, 0.0)
            inverse = unit_lower_inverse(low, row, col).astype(BF16)
            right = jnp.concatenate([key * (beta_col * jnp.exp(run_col)), value * beta_col], axis=1)
            solved = dot1(inverse, right.astype(BF16))
            rest = right - solved - dot3(low, solved)
            solved = solved + dot1(inverse, rest.astype(BF16))
            late = key * jnp.exp(last - run_col)
            made = dot3(late.T, solved)
            keep = jnp.where(row == col, jnp.exp(last), 0.0)
            maps.append(jnp.concatenate([keep - made[:, :DK], made[:, DK:]], axis=1))
        while len(maps) > 1:
            maps = [composed(maps[i], maps[i + 1]) for i in range(0, len(maps), 2)]
        (mine, other)[which][...] = maps[0]


def composed(earlier, later):
    both = dot3(later[:, :DK], earlier)
    return jnp.concatenate([both[:, :DK], both[:, DK:] + later[:, DK:]], axis=1)


def local_maps(xg, w_key, w_value, w_other, gate_rows):
    _, rows, _ = xg.shape
    used = rows - PAD
    shape = jax.ShapeDtypeStruct((DK, DK + DV), F32)
    return pl.pallas_call(
        map_kernel,
        in_specs=[VMEM] * 5,
        out_specs=[VMEM] * 2,
        out_shape=[shape] * 2,
        scratch_shapes=[
            pltpu.VMEM((2, used, DK + DV), F32),
            pltpu.VMEM((gate_rows.shape[0], used), F32),
        ],
        compiler_params=granted(24),
    )(xg, w_key, w_value, w_other, gate_rows)


def in_order(mine, other, late):
    earlier = jnp.where(late, other, mine)
    later = jnp.where(late, mine, other)
    return composed(earlier, later)


def pair_kernel(mine, other, out):
    out[...] = in_order(mine[...], other[...], lax.axis_index("tp") % 2 == 1)


def pair_composed(mine, other):
    return pl.pallas_call(
        pair_kernel,
        in_specs=[VMEM] * 2,
        out_specs=VMEM,
        out_shape=jax.ShapeDtypeStruct(mine.shape, F32),
        compiler_params=granted(4),
    )(mine, other)


QUARTER = 32


def couple_kernel(mine, other, keep, give):
    place = lax.axis_index("sp")
    whole = in_order(mine[...], other[...], place % 2 == 1)
    keep[...] = whole
    core = place % 2

    @pl.when((place // 2) % 2 == 0)
    def _():
        give[...] = whole[:, DK:]

    @pl.when((place // 2) % 2 == 1)
    def _():
        mine_rows = pl.ds(pl.multiple_of(core * QUARTER, QUARTER), QUARTER)
        give[0:QUARTER, :] = keep[mine_rows, :DK]
        give[QUARTER : 2 * QUARTER, :] = keep[mine_rows, DK:]
        give[2 * QUARTER :, :] = jnp.zeros((DK - 2 * QUARTER, DV), F32)


def coupled(mine, other):
    return pl.pallas_call(
        couple_kernel,
        in_specs=[VMEM] * 2,
        out_specs=[VMEM] * 2,
        out_shape=[jax.ShapeDtypeStruct(mine.shape, F32), jax.ShapeDtypeStruct((DK, DV), F32)],
        compiler_params=granted(4),
    )(mine, other)


def owner_kernel(keep, got, query, state, read):
    place = lax.axis_index("sp")
    late = (place // 2) % 2 == 1
    core = place % 2
    rows = pl.ds(pl.multiple_of(2 * QUARTER + core * QUARTER, QUARTER), QUARTER)
    early = jnp.where(late, got[...], keep[:, DK:])
    last_map = jnp.where(late, keep[rows, :DK], got[0:QUARTER, :])
    last_add = jnp.where(late, keep[rows, DK:], got[QUARTER : 2 * QUARTER, :])
    owned = (dot3(last_map, early) + last_add).astype(BF16)
    state[...] = owned
    which = lax.broadcasted_iota(jnp.int32, query.shape, 0)
    lane = lax.broadcasted_iota(jnp.int32, query.shape, 1)
    chosen = (which == place // 4) & (lane // QUARTER == place % 4)
    picked = jnp.where(chosen, query[...].astype(F32), 0.0).astype(BF16)
    tall = jnp.concatenate([owned] * (DK // QUARTER), axis=0)
    read[...] = jnp.sum(dot1(picked, tall), axis=0, keepdims=True)


def owner_rows(keep, got, query):
    return pl.pallas_call(
        owner_kernel,
        in_specs=[VMEM] * 3,
        out_specs=[VMEM] * 2,
        out_shape=[jax.ShapeDtypeStruct((QUARTER, DV), BF16), jax.ShapeDtypeStruct((1, DV), F32)],
        compiler_params=granted(4),
    )(keep, got, query)


def shards(
    layer_input,
    w_key,
    w_value,
    w_gates,
    decay_rate,
    beta_bias,
    log_decay_extra,
    new_query,
    read_gain,
):
    prompts, _, _ = layer_input.shape
    sp = lax.axis_size("sp")
    tp = lax.axis_size("tp")
    chunks = sp // prompts
    pair = [(i, i ^ 1) for i in range(tp)]
    w_other = lax.ppermute(jnp.stack([w_key, w_value]), "tp", pair)

    sent = packed(layer_input, log_decay_extra[:, 0, :])
    groups = [[prompts * t + j for j in range(prompts)] for t in range(chunks)]
    here = lax.all_to_all(sent, "sp", 0, 0, axis_index_groups=groups, tiled=True)

    parcel = parcels(here, decay_rate, beta_bias, tp)
    gathered = lax.all_to_all(parcel, "tp", 0, 0, tiled=True)

    gate_rows = w_gates.transpose(0, 2, 1).reshape(2 * tp, -1)
    mine, theirs = local_maps(gathered, w_key, w_value, w_other, gate_rows)
    other = lax.ppermute(theirs, "tp", pair)
    whole = pair_composed(mine, other)

    moved = lax.ppermute(
        whole, "sp", [(prompts * t + j, chunks * j + t) for t in range(chunks) for j in range(prompts)]
    )
    near = lax.ppermute(moved, "sp", [(i, i ^ 1) for i in range(sp)])
    keep, give = coupled(moved, near)
    got = lax.ppermute(give, "sp", [(i, i ^ 2) for i in range(sp)])
    state_cache, partial = owner_rows(keep, got, new_query)

    parts = lax.all_to_all(
        jnp.broadcast_to(partial[None], (sp, 1, DV)), "sp", 0, 0, tiled=True
    )
    raw = parts.reshape(prompts, chunks, DV).sum(axis=1)
    scaled = raw * lax.rsqrt(jnp.mean(raw * raw, axis=-1, keepdims=True) + EPS) * read_gain
    return state_cache, scaled.astype(BF16)


def solution(mesh):
    placed = (
        P(None, "sp", "tp"),
        P(None, "tp"),
        P(None, "tp"),
        P(),
        P("tp"),
        P("tp"),
        P(None, "tp", "sp"),
        P(None, "tp"),
        P(),
    )

    return jax.shard_map(
        shards, mesh=mesh, in_specs=placed, out_specs=(P("sp", "tp"), P(None, "tp")), check_vma=False
    )
```

time: 408 us -> 160 us (0.39)
  waiting for transfers between devices: 236 us -> 73.5 us
  other arithmetic: 82.5 us -> 0.89 us
  matrix products: 40.8 us -> 0 us
  starting transfers between devices: 10.1 us -> 37.6 us
  Pallas kernels: 0 us -> 21.8 us
  between operations: 15.5 us -> 2.07 us
    all_gather x3 -> x0, waiting for transfers between devices: 202 us -> none  [the longest x2 127 us: prefix_by_axis(): pieces = lax.all_gather(total, axis)]
    another operation x4 -> x1, other arithmetic: 79.2 us -> 0.1 us  [shards(): w_other = lax.ppermute(jnp.stack([w_key, w_value]), 'tp', pair)]
    ppermute x0 -> x5, waiting for transfers between devices: none -> 65.4 us  [the longest x1 46.5 us: shards(): w_other = lax.ppermute(jnp.stack([w_key, w_value]), 'tp', pair)]
    dot_general x31 -> x0, matrix products: 39.8 us -> none  [the longest x24 25.9 us: matmul_high(): return jnp.einsum('...ab,...bc->...ac', left, right, precision=HIGH)]
    all_to_all x1 -> x2, waiting for transfers between devices: 33.4 us -> 8.06 us  [the longest x1 8.06 us: shards(): lax.all_to_all(sent, 'sp', 0, 0, axis_index_groups=groups, tiled=True)]
    ppermute x0 -> x5, starting transfers between devices: none -> 23.4 us  [the longest x1 13.2 us: shards(): got = lax.ppermute(give, 'sp', [(i, i ^ 2) for i in range(sp)])]
    pallas_call x0 -> x6, Pallas kernels: none -> 21.8 us  [the longest x1 19.6 us: local_maps(): pl.pallas_call(map_kernel, in_specs=[VMEM] * 5, out_specs=[VMEM] * 2, out...]
    all_to_all x1 -> x2, starting transfers between devices: 9.76 us -> 14.3 us  [the longest x1 10.2 us: shards(): lax.all_to_all(sent, 'sp', 0, 0, axis_index_groups=groups, tiled=True)]
  transfers between devices with their start and end apart: 4 -> 7, of which waited for: 4 -> 6; matrix products, arithmetic and copies ran while one was open for 1% -> 0% of each run, Pallas kernels for 0% -> 0%
where the time goes in v1:
time: 160 us; the launch traced here: 159 us
  waiting for transfers between devices  73.5 us (46%)
  starting transfers between devices  37.6 us (24%)
  Pallas kernels  21.8 us (14%)
  blocking collectives  18 us (11%)
  local copies, waits for them, and re-layouts  5.21 us (3%)
  between operations  2.07 us (1%)
    ppermute x1, waiting for transfers between devices, shards(): w_other = lax.ppermute(jnp.stack([w_key, w_value]), 'tp', pair)  46.5 us
    pallas_call x1, Pallas kernels, local_maps(): pl.pallas_call(map_kernel, in_specs=[VMEM] * 5, out_specs=[VMEM] * 2, out...  19.6 us
    all_to_all x1, blocking collectives, shards(): lax.all_to_all(jnp.broadcast_to(partial[None], (sp, 1, DV)), 'sp', 0, 0,...  18 us
    ppermute x1, starting transfers between devices, shards(): got = lax.ppermute(give, 'sp', [(i, i ^ 2) for i in range(sp)])  13.2 us
    ppermute x1, waiting for transfers between devices, shards(): lax.ppermute(whole, 'sp', [(prompts * t + j, chunks * j + t) for t in ran...  11.7 us
    all_to_all x1, starting transfers between devices, shards(): lax.all_to_all(sent, 'sp', 0, 0, axis_index_groups=groups, tiled=True)  10.2 us
    all_to_all x1, waiting for transfers between devices, shards(): lax.all_to_all(sent, 'sp', 0, 0, axis_index_groups=groups, tiled=True)  8.06 us
    unnamed x20, local copies, waits for them, and re-layouts  5.2 us
  transfers between devices with their start and end apart: 7, of which 6 were waited for; matrix products, arithmetic and copies ran while one was open for 0% of the time, Pallas kernels for 0%

profile of v1, /device:TPU:1, one launch (start us, length us, event | category | flops | bytes accessed | tf_op | source)
XLA Modules:
  0.0 159.1 jit_solution(3267857668532823863)
XLA Ops:
  0.6 0.9 copy-done.5
  1.6 0.7 copy-done.7
  2.3 0.7 shard_map.104
  3.0 10.2 %all-to-all-start = ((bf16[8,144,128]{2,1,0:T(8,128)(2,1)}), bf16[8,144,128]{2,1,0:T(8,128)(2,1)S(1)}, u32[]{:S(2)}, u32[]{:S(2)}) async-start(bf16[8,144,128]{2,1,0:T(8,128)(2,1)} %shard_map.104), calls=%async_computation | async-start | bytes 589824 | tf_op jit(solution)/shard_map/all_to_all | solution.py:308
  14.5 8.1 %all-to-all-done.here = bf16[8,144,128]{2,1,0:T(8,128)(2,1)S(1)} async-done(((bf16[8,144,128]{2,1,0:T(8,128)(2,1)}), bf16[8,144,128]{2,1,0:T(8,128)(2,1)S(1)}, u32[]{:S(2)}, u32[]{:S(2)}) %all-to-all-start) | async-done | bytes 294944 | tf_op jit(solution)/shard_map/all_to_all | solution.py:308
  22.5 0.3 shard_map.105
  22.8 1.3 copy-done
  24.2 4.1 %all-to-all-start.1 = ((bf16[16,528,128]{2,1,0:T(8,128)(2,1)}), bf16[16,528,128]{2,1,0:T(8,128)(2,1)S(1)}, u32[]{:S(2)}, u32[]{:S(2)}) async-start(bf16[16,528,128]{2,1,0:T(8,128)(2,1)} %copy-done), calls=%async_computation.1 | async-start | bytes 4325376 | tf_op jit(solution)/shard_map/all_to_all | solution.py:311
  28.4 3.3 %collective-permute-start = (bf16[2,2048,128]{2,1,0:T(8,128)(2,1)S(1)}, bf16[2,2048,128]{2,1,0:T(8,128)(2,1)S(1)}, u32[]{:S(2)}, u32[]{:S(2)}) collective-permute-start(bf16[2,2048,128]{2,1,0:T(8,128)(2,1)S(1)} %pad_maximum_fusion), channel_id=1, source_target_pairs={{0,1},{1,0},{2,3},{3,2},{4,5},{5,4},{6,7},{7,6},{8,9},{9,8},{10,11... | collective-permute-start | bytes 3145736 | tf_op jit(solution)/shard_map/ppermute | solution.py:304
  31.7 46.5 %collective-permute-done.wo = bf16[2,2048,128]{2,1,0:T(8,128)(2,1)S(1)} collective-permute-done((bf16[2,2048,128]{2,1,0:T(8,128)(2,1)S(1)}, bf16[2,2048,128]{2,1,0:T(8,128)(2,1)S(1)}, u32[]{:S(2)}, u32[]{:S(2)}) %collective-permute-start) | collective-permute-done | bytes 1048608 | tf_op jit(solution)/shard_map/ppermute | solution.py:304
  78.2 1.0 copy-done.3
  79.2 1.2 copy-done.4
  80.4 19.6 %shard_map.106 = (f32[128,256]{1,0:T(8,128)S(1)}, f32[128,256]{1,0:T(8,128)S(1)}) custom-call(bf16[16,528,128]{2,1,0:T(8,128)(2,1)S(1)} %all-to-all-done.1.xg, bf16[2048,128]{1,0:T(8,128)(2,1)S(1)} %copy-done.1, bf16[2048,128]{1,0:T(8,128)(2,1)S(1)} %copy-done.2, bf16[2,2048,128]{2,1,0:T(8,128)(2,1)S(1)} %copy-done.4, bf16[32,2048]{1,0:T(8,128)(2,1)S(1)} %bitcast.10), custom_call_target="tpu_custom_call" | custom-call | tf_op jit(solution)/shard_map/pallas_call | solution.py:196
  100.0 1.9 %collective-permute-start.1 = (f32[128,256]{1,0:T(8,128)S(1)}, f32[128,256]{1,0:T(8,128)S(1)}, u32[]{:S(2)}, u32[]{:S(2)}) collective-permute-start(f32[128,256]{1,0:T(8,128)S(1)} %get-tuple-element.9), channel_id=1, source_target_pairs={{0,1},{1,0},{2,3},{3,2},{4,5},{5,4},{6,7},{7,6},{8,9},{9,8},{10,11... | collective-permute-start | bytes 393224 | tf_op jit(solution)/shard_map/ppermute | solution.py:315
  102.0 3.8 %collective-permute-done.1.other = f32[128,256]{1,0:T(8,128)S(1)} collective-permute-done((f32[128,256]{1,0:T(8,128)S(1)}, f32[128,256]{1,0:T(8,128)S(1)}, u32[]{:S(2)}, u32[]{:S(2)}) %collective-permute-start.1) | collective-permute-done | bytes 131104 | tf_op jit(solution)/shard_map/ppermute | solution.py:315
  106.0 3.1 %collective-permute-start.2 = (f32[128,256]{1,0:T(8,128)S(1)}, f32[128,256]{1,0:T(8,128)S(1)}, u32[]{:S(2)}, u32[]{:S(2)}) collective-permute-start(f32[128,256]{1,0:T(8,128)S(1)} %shard_map.107), channel_id=1, source_target_pairs={{0,0},{16,64},{32,128},{48,192},{64,256},{80,320},{96,384},{112,44... | collective-permute-start | bytes 393224 | tf_op jit(solution)/shard_map/ppermute | solution.py:318
  109.1 11.7 %collective-permute-done.2.mine = f32[128,256]{1,0:T(8,128)S(1)} collective-permute-done((f32[128,256]{1,0:T(8,128)S(1)}, f32[128,256]{1,0:T(8,128)S(1)}, u32[]{:S(2)}, u32[]{:S(2)}) %collective-permute-start.2) | collective-permute-done | bytes 131104 | tf_op jit(solution)/shard_map/ppermute | solution.py:318
  120.7 1.9 %collective-permute-start.3 = (f32[128,256]{1,0:T(8,128)S(1)}, f32[128,256]{1,0:T(8,128)S(1)}, u32[]{:S(2)}, u32[]{:S(2)}) collective-permute-start(f32[128,256]{1,0:T(8,128)S(1)} %collective-permute-done.2.mine), channel_id=1, source_target_pairs={{0,16},{16,0},{32,48},{48,32},{64,80},{80,64},{96,112},{112,96},{1... | collective-permute-start | bytes 393224 | tf_op jit(solution)/shard_map/ppermute | solution.py:321
  122.7 1.3 collective-permute-done.3.other
  124.2 13.2 %collective-permute-start.4 = (f32[128,128]{1,0:T(8,128)S(1)}, f32[128,128]{1,0:T(8,128)S(1)}, u32[]{:S(2)}, u32[]{:S(2)}) collective-permute-start(f32[128,128]{1,0:T(8,128)S(1)} %get-tuple-element.11), channel_id=1, source_target_pairs={{0,32},{16,48},{32,0},{48,16},{64,96},{80,112},{96,64},{112,80},{1... | collective-permute-start | bytes 196616 | tf_op jit(solution)/shard_map/ppermute | solution.py:323
  137.4 2.1 %collective-permute-done.4.got = f32[128,128]{1,0:T(8,128)S(1)} collective-permute-done((f32[128,128]{1,0:T(8,128)S(1)}, f32[128,128]{1,0:T(8,128)S(1)}, u32[]{:S(2)}, u32[]{:S(2)}) %collective-permute-start.4) | collective-permute-done | bytes 65568 | tf_op jit(solution)/shard_map/ppermute | solution.py:323
  139.5 0.8 shard_map.109
  140.3 18.0 %all_to_all.15 = f32[32,1,128]{2,1,0:T(1,128)S(1)} all-to-all(f32[32,1,128]{2,1,0:T(1,128)S(1)} %broadcast_in_dim.5), channel_id=1, replica_groups=mesh['sp'=32,'tp'=16] {'sp'}, dimensions={0} | all-to-all | bytes 32768 | tf_op jit(solution)/shard_map/all_to_all | solution.py:326
  158.4 0.7 multiply_convert_fusion
  (23 shorter events, 0.7 us)
Async XLA Ops:
  0.6 1.0 copy-start.5
  1.6 0.7 copy-start.7
  3.0 19.5 %all-to-all-start = ((bf16[8,144,128]{2,1,0:T(8,128)(2,1)}), bf16[8,144,128]{2,1,0:T(8,128)(2,1)S(1)}, u32[]{:S(2)}, u32[]{:S(2)}) async-start(bf16[8,144,128]{2,1,0:T(8,128)(2,1)} %shard_map.104), calls=%async_computation | async-start | bytes 589824 | tf_op jit(solution)/shard_map/all_to_all | solution.py:308
  22.8 1.4 copy-start
  24.2 4.1 %copy-start.1 = (bf16[2048,128]{1,0:T(8,128)(2,1)S(1)}, bf16[2048,128]{1,0:T(8,128)(2,1)}, u32[]{:S(2)}) copy-start(bf16[2048,128]{1,0:T(8,128)(2,1)} %wk.1) | copy-start | bytes 1572868
  24.2 4.1 %copy-start.2 = (bf16[2048,128]{1,0:T(8,128)(2,1)S(1)}, bf16[2048,128]{1,0:T(8,128)(2,1)}, u32[]{:S(2)}) copy-start(bf16[2048,128]{1,0:T(8,128)(2,1)} %wv.1) | copy-start | bytes 1572868
  24.2 55.0 %copy-start.6 = (bf16[2,2048,16]{1,2,0:T(8,128)(2,1)S(1)}, bf16[2,2048,16]{1,2,0:T(8,128)(2,1)}, u32[]{:S(2)}) copy-start(bf16[2,2048,16]{1,2,0:T(8,128)(2,1)} %param.12) | copy-start | bytes 393220
  24.2 55.0 %all-to-all-start.1 = ((bf16[16,528,128]{2,1,0:T(8,128)(2,1)}), bf16[16,528,128]{2,1,0:T(8,128)(2,1)S(1)}, u32[]{:S(2)}, u32[]{:S(2)}) async-start(bf16[16,528,128]{2,1,0:T(8,128)(2,1)} %copy-done), calls=%async_computation.1 | async-start | bytes 4325376 | tf_op jit(solution)/shard_map/all_to_all | solution.py:311
  28.4 49.8 %collective-permute-start = (bf16[2,2048,128]{2,1,0:T(8,128)(2,1)S(1)}, bf16[2,2048,128]{2,1,0:T(8,128)(2,1)S(1)}, u32[]{:S(2)}, u32[]{:S(2)}) collective-permute-start(bf16[2,2048,128]{2,1,0:T(8,128)(2,1)S(1)} %pad_maximum_fusion), channel_id=1, source_target_pairs={{0,1},{1,0},{2,3},{3,2},{4,5},{5,4},{6,7},{7,6},{8,9},{9,8},{10,11... | collective-permute-start | bytes 3145736 | tf_op jit(solution)/shard_map/ppermute | solution.py:304
  78.2 1.0 copy-start.3
  79.2 1.2 copy-start.4
  80.4 59.1 %copy-start.8 = (bf16[8,128]{1,0:T(8,128)(2,1)S(1)}, bf16[8,128]{1,0:T(8,128)(2,1)}, u32[]{:S(2)}) copy-start(bf16[8,128]{1,0:T(8,128)(2,1)} %query.1) | copy-start | bytes 6148
  80.4 78.0 %copy-start.9 = (f32[128]{0:T(128)S(1)}, f32[128]{0:T(128)}, u32[]{:S(2)}) copy-start(f32[128]{0:T(128)} %param.17) | copy-start | bytes 1540
  100.0 5.7 %collective-permute-start.1 = (f32[128,256]{1,0:T(8,128)S(1)}, f32[128,256]{1,0:T(8,128)S(1)}, u32[]{:S(2)}, u32[]{:S(2)}) collective-permute-start(f32[128,256]{1,0:T(8,128)S(1)} %get-tuple-element.9), channel_id=1, source_target_pairs={{0,1},{1,0},{2,3},{3,2},{4,5},{5,4},{6,7},{7,6},{8,9},{9,8},{10,11... | collective-permute-start | bytes 393224 | tf_op jit(solution)/shard_map/ppermute | solution.py:315
  106.0 14.8 %collective-permute-start.2 = (f32[128,256]{1,0:T(8,128)S(1)}, f32[128,256]{1,0:T(8,128)S(1)}, u32[]{:S(2)}, u32[]{:S(2)}) collective-permute-start(f32[128,256]{1,0:T(8,128)S(1)} %shard_map.107), channel_id=1, source_target_pairs={{0,0},{16,64},{32,128},{48,192},{64,256},{80,320},{96,384},{112,44... | collective-permute-start | bytes 393224 | tf_op jit(solution)/shard_map/ppermute | solution.py:318
  120.7 3.2 %collective-permute-start.3 = (f32[128,256]{1,0:T(8,128)S(1)}, f32[128,256]{1,0:T(8,128)S(1)}, u32[]{:S(2)}, u32[]{:S(2)}) collective-permute-start(f32[128,256]{1,0:T(8,128)S(1)} %collective-permute-done.2.mine), channel_id=1, source_target_pairs={{0,16},{16,0},{32,48},{48,32},{64,80},{80,64},{96,112},{112,96},{1... | collective-permute-start | bytes 393224 | tf_op jit(solution)/shard_map/ppermute | solution.py:321
  124.2 15.3 %collective-permute-start.4 = (f32[128,128]{1,0:T(8,128)S(1)}, f32[128,128]{1,0:T(8,128)S(1)}, u32[]{:S(2)}, u32[]{:S(2)}) collective-permute-start(f32[128,128]{1,0:T(8,128)S(1)} %get-tuple-element.11), channel_id=1, source_target_pairs={{0,32},{16,48},{32,0},{48,16},{64,96},{80,112},{96,64},{112,80},{1... | collective-permute-start | bytes 196616 | tf_op jit(solution)/shard_map/ppermute | solution.py:323

commit v2 on v1

--- a/solution.py
+++ b/solution.py
@@ -14,6 +14,7 @@
 F32 = jnp.float32
 BF16 = jnp.bfloat16
 PAD = 16
+SHIFT = 5
 
 
 MIB = 1 << 20
@@ -40,26 +41,44 @@
 
 
 def dot3(left, right, dims=NN):
-    lh, ll = left if isinstance(left, tuple) else halves(left)
-    rh, rl = right if isinstance(right, tuple) else halves(right)
-    return dot1(lh, rh, dims) + (dot1(ll, rh, dims) + dot1(lh, rl, dims))
-
-
-def unit_lower_inverse(low, row, col):
-    size = low.shape[0]
-    eye = (row == col).astype(F32)
-    step = 1
-    inverse = eye
-    while step < size:
-        merge = ((row // (2 * step)) == (col // (2 * step))) & ((row // step) != (col // step))
-        part = jnp.where(merge, low, 0.0)
-        if step == 1:
-            inverse = eye - part
-        else:
-            held = inverse.astype(BF16)
-            inverse = inverse - dot1(dot1(held, part.astype(BF16)).astype(BF16), held)
-        step *= 2
-    return inverse
+    (la,), (ra,) = dims[0]
+    lh, ll = halves(left)
+    rh, rl = halves(right)
+    return dot1(
+        jnp.concatenate([lh, ll, lh], axis=la), jnp.concatenate([rh, rh, rl], axis=ra), dims
+    )
+
+
+MIB = 1 << 20
+VMEM = pl.BlockSpec(memory_space=pltpu.VMEM)
+SMEM = pl.BlockSpec(memory_space=pltpu.SMEM)
+
+
+def granted(mib):
+    return pltpu.CompilerParams(vmem_limit_bytes=mib * MIB)
+
+
+NN = (((1,), (0,)), ((), ()))
+NT = (((1,), (1,)), ((), ()))
+
+
+def dot1(left, right, dims=NN):
+    return lax.dot_general(left, right, dims, preferred_element_type=F32)
+
+
+def halves(x):
+    high = x.astype(BF16)
+    low = (x - high.astype(F32)).astype(BF16)
+    return high, low
+
+
+def dot3(left, right, dims=NN):
+    (la,), (ra,) = dims[0]
+    lh, ll = halves(left)
+    rh, rl = halves(right)
+    return dot1(
+        jnp.concatenate([lh, ll, lh], axis=la), jnp.concatenate([rh, rh, rl], axis=ra), dims
+    )
 
 
 def three_pieces(x):
@@ -71,11 +90,12 @@
 
 def pack_kernel(x, extra, out):
     prompts, seg, width = x.shape
-    out[:, :seg, :] = x[...]
-    pieces = three_pieces(extra[...])
-    for p in range(prompts):
-        rows = [piece[p : p + 1] for piece in pieces] + [jnp.zeros((PAD - 3, width), F32)]
-        out[p, seg:, :] = jnp.concatenate(rows, axis=0).astype(BF16)
+    first = lax.axis_index("sp") // prompts * 2 + SHIFT
+    for i in range(prompts):
+        prompt = lax.rem(first + i, prompts)
+        out[i, :seg, :] = x[prompt]
+        rows = list(three_pieces(extra[pl.ds(prompt, 1), :])) + [jnp.zeros((PAD - 3, width), F32)]
+        out[i, seg:, :] = jnp.concatenate(rows, axis=0).astype(BF16)
 
 
 def packed(layer_input, extra):
@@ -118,19 +138,53 @@
     )(here, rate, bias)
 
 
-def map_kernel(xg, wk, wv, wo, wg, mine, other, acc, gates):
+def invert_unit_lower(low, inverse, product, row, col):
+    units, size, _ = low.shape
+    step = 1
+    while step < size:
+        merge = ((row // (2 * step)) == (col // (2 * step))) & ((row // step) != (col // step))
+        if step == 1:
+            eye = (row == col).astype(F32)
+            for u in range(units):
+                part = jnp.where(merge, low[u].astype(F32), 0.0)
+                inverse[u] = (eye - part).astype(BF16)
+        else:
+            if step < 16:
+                lower_rows = [(0, size)]
+            else:
+                lower_rows = [(at, step) for at in range(step, size, 2 * step)]
+            rows = sum(length for _, length in lower_rows)
+            take = lambda u: jnp.concatenate([inverse[u, at : at + n, :] for at, n in lower_rows], axis=0)
+            for u in range(units):
+                part = jnp.where(merge, low[u].astype(F32), 0.0).astype(BF16)
+                product[u, :rows, :] = dot1(take(u), part).astype(BF16)
+            for u in range(units):
+                fill = dot1(product[u, :rows, :], inverse[u])
+                fill = (take(u).astype(F32) - fill).astype(BF16)
+                done = 0
+                for at, n in lower_rows:
+                    inverse[u, at : at + n, :] = fill[done : done + n]
+                    done += n
+        step *= 2
+
+
+def map_kernel(
+    xg, wk, wv, wok, wov, wg, mine, other, acc, gates, keys, low, low_rest, inverse, product, right, solved, maps
+):
     sources, rows, width = xg.shape
     rows = rows - PAD
     blocks = rows // BLOCK
+    units = 2 * blocks
     me = lax.axis_index("tp")
     x = jnp.concatenate([xg[i, :rows, :] for i in range(sources)], axis=1)
+    gates[...] = dot1(wg[...], x, NT)
     acc[0] = dot1(x, jnp.concatenate([wk[...], wv[...]], axis=1))
-    acc[1] = dot1(x, jnp.concatenate([wo[0], wo[1]], axis=1))
-    gates[...] = dot1(wg[...], x, NT)
+    acc[1] = dot1(x, jnp.concatenate([wok[...], wov[...]], axis=1))
 
     row = lax.broadcasted_iota(jnp.int32, (BLOCK, BLOCK), 0)
     col = lax.broadcasted_iota(jnp.int32, (BLOCK, BLOCK), 1)
     upto = (row <= col).astype(F32)
+    strict = row > col
     decays, betas = [], []
     for which in range(2):
         head = me if which == 0 else me ^ 1
@@ -150,38 +204,55 @@
         jnp.concatenate(decays, axis=0), upto, precision=HIGH, preferred_element_type=F32
     )
     beta = jnp.concatenate(betas, axis=0)
-    units = 2 * blocks
     tall = jnp.concatenate([running, beta, jnp.zeros((BLOCK - 2 * units, BLOCK), F32)], axis=0)
     columns = tall.T
-    for which in range(2):
-        maps = []
-        for b in range(blocks):
-            u = which * blocks + b
-            pre = acc[which, BLOCK * b : BLOCK * (b + 1), :]
-            act = pre * jax.nn.sigmoid(pre)
-            key, value = act[:, :DK], act[:, DK:]
-            key = key * lax.rsqrt(jnp.sum(key * key, axis=1, keepdims=True) + EPS)
-            run_row = jnp.broadcast_to(running[u : u + 1, :], (BLOCK, BLOCK))
-            run_col = jnp.broadcast_to(columns[:, u : u + 1], (BLOCK, BLOCK))
-            beta_col = jnp.broadcast_to(columns[:, units + u : units + u + 1], (BLOCK, BLOCK))
-            last = jnp.broadcast_to(running[u : u + 1, BLOCK - 1 :], (BLOCK, BLOCK))
-            split = halves(key)
-            gram = dot3(split, split, NT)
-            strict = row > col
-            weights = jnp.exp(jnp.where(strict, run_col - run_row, 0.0))
-            low = jnp.where(strict, gram * beta_col * weights, 0.0)
-            inverse = unit_lower_inverse(low, row, col).astype(BF16)
-            right = jnp.concatenate([key * (beta_col * jnp.exp(run_col)), value * beta_col], axis=1)
-            solved = dot1(inverse, right.astype(BF16))
-            rest = right - solved - dot3(low, solved)
-            solved = solved + dot1(inverse, rest.astype(BF16))
-            late = key * jnp.exp(last - run_col)
-            made = dot3(late.T, solved)
-            keep = jnp.where(row == col, jnp.exp(last), 0.0)
-            maps.append(jnp.concatenate([keep - made[:, :DK], made[:, DK:]], axis=1))
-        while len(maps) > 1:
-            maps = [composed(maps[i], maps[i + 1]) for i in range(0, len(maps), 2)]
-        (mine, other)[which][...] = maps[0]
+    run_col = lambda u: jnp.broadcast_to(columns[:, u : u + 1], (BLOCK, BLOCK))
+    beta_col = lambda u: jnp.broadcast_to(columns[:, units + u : units + u + 1], (BLOCK, BLOCK))
+    run_row = lambda u: jnp.broadcast_to(running[u : u + 1, :], (BLOCK, BLOCK))
+    last = lambda u: jnp.broadcast_to(running[u : u + 1, BLOCK - 1 :], (BLOCK, BLOCK))
+    for u in range(units):
+        which, b = divmod(u, blocks)
+        pre = acc[which, BLOCK * b : BLOCK * (b + 1), :]
+        act = pre * jax.nn.sigmoid(pre)
+        key, value = act[:, :DK], act[:, DK:]
+        key = key * lax.rsqrt(jnp.sum(key * key, axis=1, keepdims=True) + EPS)
+        keys[u] = key
+        strength = beta_col(u)
+        right[u, :, :DK] = key * (strength * jnp.exp(run_col(u)))
+        right[u, :, DK:] = value * strength
+    for u in range(units):
+        key = keys[u]
+        gram = dot3(key, key, NT)
+        weights = jnp.exp(jnp.where(strict, run_col(u) - run_row(u), 0.0))
+        high, rest = halves(jnp.where(strict, gram * beta_col(u) * weights, 0.0))
+        low[u] = high
+        low_rest[u] = rest
+    invert_unit_lower(low, inverse, product, row, col)
+    for u in range(units):
+        solved[u] = dot1(inverse[u], right[u].astype(BF16)).astype(BF16)
+    for u in range(units):
+        first = solved[u]
+        taken = dot1(
+            jnp.concatenate([low[u], low_rest[u]], axis=1), jnp.concatenate([first, first], axis=0)
+        )
+        right[u] = right[u] - first.astype(F32) - taken
+    for u in range(units):
+        right[u] = solved[u].astype(F32) + dot1(inverse[u], right[u].astype(BF16))
+    for u in range(units):
+        late = keys[u] * jnp.exp(last(u) - run_col(u))
+        made = dot3(late.T, right[u])
+        keep = jnp.where(row == col, jnp.exp(last(u)), 0.0)
+        maps[u, :, :DK] = keep - made[:, :DK]
+        maps[u, :, DK:] = made[:, DK:]
+    apart = 1
+    while apart < blocks:
+        for u in range(0, units, 2 * apart):
+            result = composed(maps[u], maps[u + apart])
+            if 2 * apart < blocks:
+                maps[u] = result
+            else:
+                (mine, other)[u // blocks][...] = result
+        apart *= 2
 
 
 def composed(earlier, later):
@@ -189,21 +260,30 @@
     return jnp.concatenate([both[:, :DK], both[:, DK:] + later[:, DK:]], axis=1)
 
 
-def local_maps(xg, w_key, w_value, w_other, gate_rows):
+def local_maps(xg, w_key, w_value, other_key, other_value, gate_rows):
     _, rows, _ = xg.shape
     used = rows - PAD
+    units = 2 * (used // BLOCK)
     shape = jax.ShapeDtypeStruct((DK, DK + DV), F32)
     return pl.pallas_call(
         map_kernel,
-        in_specs=[VMEM] * 5,
+        in_specs=[VMEM] * 6,
         out_specs=[VMEM] * 2,
         out_shape=[shape] * 2,
         scratch_shapes=[
             pltpu.VMEM((2, used, DK + DV), F32),
             pltpu.VMEM((gate_rows.shape[0], used), F32),
+            pltpu.VMEM((units, BLOCK, DK), F32),
+            pltpu.VMEM((units, BLOCK, BLOCK), BF16),
+            pltpu.VMEM((units, BLOCK, BLOCK), BF16),
+            pltpu.VMEM((units, BLOCK, BLOCK), BF16),
+            pltpu.VMEM((units, BLOCK, BLOCK), BF16),
+            pltpu.VMEM((units, BLOCK, DK + DV), F32),
+            pltpu.VMEM((units, BLOCK, DK + DV), BF16),
+            pltpu.VMEM((units, DK, DK + DV), F32),
         ],
-        compiler_params=granted(24),
-    )(xg, w_key, w_value, w_other, gate_rows)
+        compiler_params=granted(28),
+    )(xg, w_key, w_value, other_key, other_value, gate_rows)
 
 
 def in_order(mine, other, late):
@@ -301,7 +381,8 @@
     tp = lax.axis_size("tp")
     chunks = sp // prompts
     pair = [(i, i ^ 1) for i in range(tp)]
-    w_other = lax.ppermute(jnp.stack([w_key, w_value]), "tp", pair)
+    other_key = lax.ppermute(w_key, "tp", pair)
+    other_value = lax.ppermute(w_value, "tp", pair)
 
     sent = packed(layer_input, log_decay_extra[:, 0, :])
     groups = [[prompts * t + j for j in range(prompts)] for t in range(chunks)]
@@ -311,13 +392,16 @@
     gathered = lax.all_to_all(parcel, "tp", 0, 0, tiled=True)
 
     gate_rows = w_gates.transpose(0, 2, 1).reshape(2 * tp, -1)
-    mine, theirs = local_maps(gathered, w_key, w_value, w_other, gate_rows)
+    mine, theirs = local_maps(gathered, w_key, w_value, other_key, other_value, gate_rows)
     other = lax.ppermute(theirs, "tp", pair)
     whole = pair_composed(mine, other)
 
-    moved = lax.ppermute(
-        whole, "sp", [(prompts * t + j, chunks * j + t) for t in range(chunks) for j in range(prompts)]
-    )
+    ways = [
+        (prompts * t + i, chunks * ((2 * t + SHIFT + i) % prompts) + t)
+        for t in range(chunks)
+        for i in range(prompts)
+    ]
+    moved = lax.ppermute(whole, "sp", ways)
     near = lax.ppermute(moved, "sp", [(i, i ^ 1) for i in range(sp)])
     keep, give = coupled(moved, near)
     got = lax.ppermute(give, "sp", [(i, i ^ 2) for i in range(sp)])

time: 160 us -> 144 us (0.900)
  Pallas kernels: 21.8 us -> 7.86 us
  waiting for transfers between devices: 73.5 us -> 62.8 us
  blocking collectives: 18 us -> 23.8 us
  starting transfers between devices: 37.6 us -> 39.8 us
    pallas_call x1, Pallas kernels: 19.6 us -> 5.69 us  [local_maps(): pl.pallas_call(map_kernel, in_specs=[VMEM] * 6, out_specs=[VMEM] * 2, out...]
    ppermute x2 -> x3, starting transfers between devices: 6.35 us -> 18.4 us  [the longest x1 13.1 us: shards(): moved = lax.ppermute(whole, 'sp', ways)]
    ppermute x2 -> x3, waiting for transfers between devices: 58.2 us -> 47.6 us  [the longest x1 33.4 us: shards(): other_key = lax.ppermute(w_key, 'tp', pair)]
    ppermute x1, starting transfers between devices: 13.2 us -> 3.3 us  [shards(): got = lax.ppermute(give, 'sp', [(i, i ^ 2) for i in range(sp)])]
    all_to_all x1, blocking collectives: 18 us -> 23.8 us  [shards(): lax.all_to_all(jnp.broadcast_to(partial[None], (sp, 1, DV)), 'sp', 0, 0,...]
    unnamed x20 -> x24, local copies, waits for them, and re-layouts: 5.2 us -> 6.64 us
  transfers between devices with their start and end apart: 7 -> 8, of which waited for: 6 -> 7; matrix products, arithmetic and copies ran while one was open for 0% -> 0% of each run, Pallas kernels for 0% -> 0%
where the time goes in v2:
time: 144 us
  waiting for transfers between devices  62.8 us (44%)
  starting transfers between devices  39.8 us (28%)
  blocking collectives  23.8 us (17%)
  Pallas kernels  7.86 us (5%)
  local copies, waits for them, and re-layouts  6.65 us (5%)
  between operations  2.07 us (1%)
    ppermute x1, waiting for transfers between devices, shards(): other_key = lax.ppermute(w_key, 'tp', pair)  33.4 us
    all_to_all x1, blocking collectives, shards(): lax.all_to_all(jnp.broadcast_to(partial[None], (sp, 1, DV)), 'sp', 0, 0,...  23.8 us
    ppermute x1, starting transfers between devices, shards(): moved = lax.ppermute(whole, 'sp', ways)  13.1 us
    ppermute x1, waiting for transfers between devices, shards(): other_value = lax.ppermute(w_value, 'tp', pair)  10.4 us
    all_to_all x1, starting transfers between devices, shards(): lax.all_to_all(sent, 'sp', 0, 0, axis_index_groups=groups, tiled=True)  10.2 us
    all_to_all x1, waiting for transfers between devices, shards(): lax.all_to_all(sent, 'sp', 0, 0, axis_index_groups=groups, tiled=True)  8.06 us
    unnamed x24, local copies, waits for them, and re-layouts  6.64 us
    pallas_call x1, Pallas kernels, local_maps(): pl.pallas_call(map_kernel, in_specs=[VMEM] * 6, out_specs=[VMEM] * 2, out...  5.69 us
  transfers between devices with their start and end apart: 8, of which 7 were waited for; matrix products, arithmetic and copies ran while one was open for 0% of the time, Pallas kernels for 0%

profile of v2, /device:TPU:1, one launch (start us, length us, event | category | flops | bytes accessed | tf_op | source)
XLA Modules:
  0.0 143.8 jit_solution(6498088467983193468)
XLA Ops:
  0.6 0.9 copy-done.7
  3.0 10.2 %all-to-all-start = ((bf16[8,144,128]{2,1,0:T(8,128)(2,1)}), bf16[8,144,128]{2,1,0:T(8,128)(2,1)S(1)}, u32[]{:S(2)}, u32[]{:S(2)}) async-start(bf16[8,144,128]{2,1,0:T(8,128)(2,1)} %shard_map.104), calls=%async_computation | async-start | bytes 589824 | tf_op jit(solution)/shard_map/all_to_all | solution.py:389
  14.5 8.1 %all-to-all-done.here = bf16[8,144,128]{2,1,0:T(8,128)(2,1)S(1)} async-done(((bf16[8,144,128]{2,1,0:T(8,128)(2,1)}), bf16[8,144,128]{2,1,0:T(8,128)(2,1)S(1)}, u32[]{:S(2)}, u32[]{:S(2)}) %all-to-all-start) | async-done | bytes 294944 | tf_op jit(solution)/shard_map/all_to_all | solution.py:389
  22.8 1.3 copy-done
  24.2 4.1 %all-to-all-start.1 = ((bf16[16,528,128]{2,1,0:T(8,128)(2,1)}), bf16[16,528,128]{2,1,0:T(8,128)(2,1)S(1)}, u32[]{:S(2)}, u32[]{:S(2)}) async-start(bf16[16,528,128]{2,1,0:T(8,128)(2,1)} %copy-done), calls=%async_computation.1 | async-start | bytes 4325376 | tf_op jit(solution)/shard_map/all_to_all | solution.py:392
  28.3 3.3 %collective-permute-start = (bf16[2048,128]{1,0:T(8,128)(2,1)S(1)}, bf16[2048,128]{1,0:T(8,128)(2,1)S(1)}, u32[]{:S(2)}, u32[]{:S(2)}) collective-permute-start(bf16[2048,128]{1,0:T(8,128)(2,1)S(1)} %copy-done.1), channel_id=1, source_target_pairs={{0,1},{1,0},{2,3},{3,2},{4,5},{5,4},{6,7},{7,6},{8,9},{9,8},{10,11... | collective-permute-start | bytes 1572872 | tf_op jit(solution)/shard_map/ppermute | solution.py:384
  31.6 2.0 %collective-permute-start.1 = (bf16[2048,128]{1,0:T(8,128)(2,1)S(1)}, bf16[2048,128]{1,0:T(8,128)(2,1)S(1)}, u32[]{:S(2)}, u32[]{:S(2)}) collective-permute-start(bf16[2048,128]{1,0:T(8,128)(2,1)S(1)} %copy-done.2), channel_id=1, source_target_pairs={{0,1},{1,0},{2,3},{3,2},{4,5},{5,4},{6,7},{7,6},{8,9},{9,8},{10,11... | collective-permute-start | bytes 1572872 | tf_op jit(solution)/shard_map/ppermute | solution.py:385
  33.6 33.4 %collective-permute-done.wok = bf16[2048,128]{1,0:T(8,128)(2,1)S(1)} collective-permute-done((bf16[2048,128]{1,0:T(8,128)(2,1)S(1)}, bf16[2048,128]{1,0:T(8,128)(2,1)S(1)}, u32[]{:S(2)}, u32[]{:S(2)}) %collective-permute-start) | collective-permute-done | bytes 524320 | tf_op jit(solution)/shard_map/ppermute | solution.py:384
  67.0 0.8 copy-done.3
  67.7 10.4 %collective-permute-done.1.wov = bf16[2048,128]{1,0:T(8,128)(2,1)S(1)} collective-permute-done((bf16[2048,128]{1,0:T(8,128)(2,1)S(1)}, bf16[2048,128]{1,0:T(8,128)(2,1)S(1)}, u32[]{:S(2)}, u32[]{:S(2)}) %collective-permute-start.1) | collective-permute-done | bytes 524320 | tf_op jit(solution)/shard_map/ppermute | solution.py:385
  78.2 0.8 copy-done.5
  79.0 1.0 copy-done.4
  80.0 1.0 copy-done.6
  81.1 5.7 %shard_map.106 = (f32[128,256]{1,0:T(8,128)S(1)}, f32[128,256]{1,0:T(8,128)S(1)}) custom-call(bf16[16,528,128]{2,1,0:T(8,128)(2,1)S(1)} %all-to-all-done.1.xg, bf16[2048,128]{1,0:T(8,128)(2,1)S(1)} %copy-done.1, bf16[2048,128]{1,0:T(8,128)(2,1)S(1)} %copy-done.2, bf16[2048,128]{1,0:T(8,128)(2,1)S(1)} %copy-done.4, bf16[2048,128]{1,0:T(8,128)(2,1)S(1)} %copy-done.6, ...), custom_call_target="tpu_custom_call" | custom-call | tf_op jit(solution)/shard_map/pallas_call | solution.py:268
  86.8 1.9 %collective-permute-start.2 = (f32[128,256]{1,0:T(8,128)S(1)}, f32[128,256]{1,0:T(8,128)S(1)}, u32[]{:S(2)}, u32[]{:S(2)}) collective-permute-start(f32[128,256]{1,0:T(8,128)S(1)} %get-tuple-element.9), channel_id=1, source_target_pairs={{0,1},{1,0},{2,3},{3,2},{4,5},{5,4},{6,7},{7,6},{8,9},{9,8},{10,11... | collective-permute-start | bytes 393224 | tf_op jit(solution)/shard_map/ppermute | solution.py:396
  88.7 3.8 %collective-permute-done.2.other = f32[128,256]{1,0:T(8,128)S(1)} collective-permute-done((f32[128,256]{1,0:T(8,128)S(1)}, f32[128,256]{1,0:T(8,128)S(1)}, u32[]{:S(2)}, u32[]{:S(2)}) %collective-permute-start.2) | collective-permute-done | bytes 131104 | tf_op jit(solution)/shard_map/ppermute | solution.py:396
  92.7 13.1 %collective-permute-start.3 = (f32[128,256]{1,0:T(8,128)S(1)}, f32[128,256]{1,0:T(8,128)S(1)}, u32[]{:S(2)}, u32[]{:S(2)}) collective-permute-start(f32[128,256]{1,0:T(8,128)S(1)} %shard_map.107), channel_id=1, source_target_pairs={{0,320},{16,384},{32,448},{48,0},{64,64},{80,128},{96,192},{112,25... | collective-permute-start | bytes 393224 | tf_op jit(solution)/shard_map/ppermute | solution.py:404
  105.8 3.8 %collective-permute-done.3.mine = f32[128,256]{1,0:T(8,128)S(1)} collective-permute-done((f32[128,256]{1,0:T(8,128)S(1)}, f32[128,256]{1,0:T(8,128)S(1)}, u32[]{:S(2)}, u32[]{:S(2)}) %collective-permute-start.3) | collective-permute-done | bytes 131104 | tf_op jit(solution)/shard_map/ppermute | solution.py:404
  109.6 1.9 %collective-permute-start.4 = (f32[128,256]{1,0:T(8,128)S(1)}, f32[128,256]{1,0:T(8,128)S(1)}, u32[]{:S(2)}, u32[]{:S(2)}) collective-permute-start(f32[128,256]{1,0:T(8,128)S(1)} %collective-permute-done.3.mine), channel_id=1, source_target_pairs={{0,16},{16,0},{32,48},{48,32},{64,80},{80,64},{96,112},{112,96},{1... | collective-permute-start | bytes 393224 | tf_op jit(solution)/shard_map/ppermute | solution.py:405
  111.5 1.3 collective-permute-done.4.other
  113.0 3.3 %collective-permute-start.5 = (f32[128,128]{1,0:T(8,128)S(1)}, f32[128,128]{1,0:T(8,128)S(1)}, u32[]{:S(2)}, u32[]{:S(2)}) collective-permute-start(f32[128,128]{1,0:T(8,128)S(1)} %get-tuple-element.11), channel_id=1, source_target_pairs={{0,32},{16,48},{32,0},{48,16},{64,96},{80,112},{96,64},{112,80},{1... | collective-permute-start | bytes 196616 | tf_op jit(solution)/shard_map/ppermute | solution.py:407
  116.3 2.1 %collective-permute-done.5.got = f32[128,128]{1,0:T(8,128)S(1)} collective-permute-done((f32[128,128]{1,0:T(8,128)S(1)}, f32[128,128]{1,0:T(8,128)S(1)}, u32[]{:S(2)}, u32[]{:S(2)}) %collective-permute-start.5) | collective-permute-done | bytes 65568 | tf_op jit(solution)/shard_map/ppermute | solution.py:407
  118.4 0.8 shard_map.109
  119.2 23.8 %all_to_all.15 = f32[32,1,128]{2,1,0:T(1,128)S(1)} all-to-all(f32[32,1,128]{2,1,0:T(1,128)S(1)} %broadcast_in_dim.5), channel_id=1, replica_groups=mesh['sp'=32,'tp'=16] {'sp'}, dimensions={0} | all-to-all | bytes 32768 | tf_op jit(solution)/shard_map/all_to_all | solution.py:410
  (28 shorter events, 2.9 us)
Async XLA Ops:
  0.6 1.0 copy-start.7
  1.6 0.7 copy-start.9
  3.0 19.5 %all-to-all-start = ((bf16[8,144,128]{2,1,0:T(8,128)(2,1)}), bf16[8,144,128]{2,1,0:T(8,128)(2,1)S(1)}, u32[]{:S(2)}, u32[]{:S(2)}) async-start(bf16[8,144,128]{2,1,0:T(8,128)(2,1)} %shard_map.104), calls=%async_computation | async-start | bytes 589824 | tf_op jit(solution)/shard_map/all_to_all | solution.py:389
  22.8 1.3 copy-start
  24.2 4.1 %copy-start.1 = (bf16[2048,128]{1,0:T(8,128)(2,1)S(1)}, bf16[2048,128]{1,0:T(8,128)(2,1)}, u32[]{:S(2)}) copy-start(bf16[2048,128]{1,0:T(8,128)(2,1)} %wk.1) | copy-start | bytes 1572868
  24.2 7.4 %copy-start.2 = (bf16[2048,128]{1,0:T(8,128)(2,1)S(1)}, bf16[2048,128]{1,0:T(8,128)(2,1)}, u32[]{:S(2)}) copy-start(bf16[2048,128]{1,0:T(8,128)(2,1)} %wv.1) | copy-start | bytes 1572868
  24.2 54.8 %copy-start.8 = (bf16[2,2048,16]{1,2,0:T(8,128)(2,1)S(1)}, bf16[2,2048,16]{1,2,0:T(8,128)(2,1)}, u32[]{:S(2)}) copy-start(bf16[2,2048,16]{1,2,0:T(8,128)(2,1)} %param.12) | copy-start | bytes 393220
  24.2 54.8 %all-to-all-start.1 = ((bf16[16,528,128]{2,1,0:T(8,128)(2,1)}), bf16[16,528,128]{2,1,0:T(8,128)(2,1)S(1)}, u32[]{:S(2)}, u32[]{:S(2)}) async-start(bf16[16,528,128]{2,1,0:T(8,128)(2,1)} %copy-done), calls=%async_computation.1 | async-start | bytes 4325376 | tf_op jit(solution)/shard_map/all_to_all | solution.py:392
  28.3 38.7 %collective-permute-start = (bf16[2048,128]{1,0:T(8,128)(2,1)S(1)}, bf16[2048,128]{1,0:T(8,128)(2,1)S(1)}, u32[]{:S(2)}, u32[]{:S(2)}) collective-permute-start(bf16[2048,128]{1,0:T(8,128)(2,1)S(1)} %copy-done.1), channel_id=1, source_target_pairs={{0,1},{1,0},{2,3},{3,2},{4,5},{5,4},{6,7},{7,6},{8,9},{9,8},{10,11... | collective-permute-start | bytes 1572872 | tf_op jit(solution)/shard_map/ppermute | solution.py:384
  31.6 46.6 %collective-permute-start.1 = (bf16[2048,128]{1,0:T(8,128)(2,1)S(1)}, bf16[2048,128]{1,0:T(8,128)(2,1)S(1)}, u32[]{:S(2)}, u32[]{:S(2)}) collective-permute-start(bf16[2048,128]{1,0:T(8,128)(2,1)S(1)} %copy-done.2), channel_id=1, source_target_pairs={{0,1},{1,0},{2,3},{3,2},{4,5},{5,4},{6,7},{7,6},{8,9},{9,8},{10,11... | collective-permute-start | bytes 1572872 | tf_op jit(solution)/shard_map/ppermute | solution.py:385
  67.0 0.8 copy-start.3
  78.2 0.8 copy-start.5
  79.0 1.0 copy-start.4
  80.0 1.0 copy-start.6
  81.1 37.4 %copy-start.10 = (bf16[8,128]{1,0:T(8,128)(2,1)S(1)}, bf16[8,128]{1,0:T(8,128)(2,1)}, u32[]{:S(2)}) copy-start(bf16[8,128]{1,0:T(8,128)(2,1)} %query.1) | copy-start | bytes 6148
  81.1 62.1 %copy-start.11 = (f32[128]{0:T(128)S(1)}, f32[128]{0:T(128)}, u32[]{:S(2)}) copy-start(f32[128]{0:T(128)} %param.17) | copy-start | bytes 1540
  86.8 5.7 %collective-permute-start.2 = (f32[128,256]{1,0:T(8,128)S(1)}, f32[128,256]{1,0:T(8,128)S(1)}, u32[]{:S(2)}, u32[]{:S(2)}) collective-permute-start(f32[128,256]{1,0:T(8,128)S(1)} %get-tuple-element.9), channel_id=1, source_target_pairs={{0,1},{1,0},{2,3},{3,2},{4,5},{5,4},{6,7},{7,6},{8,9},{9,8},{10,11... | collective-permute-start | bytes 393224 | tf_op jit(solution)/shard_map/ppermute | solution.py:396
  92.7 16.9 %collective-permute-start.3 = (f32[128,256]{1,0:T(8,128)S(1)}, f32[128,256]{1,0:T(8,128)S(1)}, u32[]{:S(2)}, u32[]{:S(2)}) collective-permute-start(f32[128,256]{1,0:T(8,128)S(1)} %shard_map.107), channel_id=1, source_target_pairs={{0,320},{16,384},{32,448},{48,0},{64,64},{80,128},{96,192},{112,25... | collective-permute-start | bytes 393224 | tf_op jit(solution)/shard_map/ppermute | solution.py:404
  109.6 3.2 %collective-permute-start.4 = (f32[128,256]{1,0:T(8,128)S(1)}, f32[128,256]{1,0:T(8,128)S(1)}, u32[]{:S(2)}, u32[]{:S(2)}) collective-permute-start(f32[128,256]{1,0:T(8,128)S(1)} %collective-permute-done.3.mine), channel_id=1, source_target_pairs={{0,16},{16,0},{32,48},{48,32},{64,80},{80,64},{96,112},{112,96},{1... | collective-permute-start | bytes 393224 | tf_op jit(solution)/shard_map/ppermute | solution.py:405
  113.0 5.4 %collective-permute-start.5 = (f32[128,128]{1,0:T(8,128)S(1)}, f32[128,128]{1,0:T(8,128)S(1)}, u32[]{:S(2)}, u32[]{:S(2)}) collective-permute-start(f32[128,128]{1,0:T(8,128)S(1)} %get-tuple-element.11), channel_id=1, source_target_pairs={{0,32},{16,48},{32,0},{48,16},{64,96},{80,112},{96,64},{112,80},{1... | collective-permute-start | bytes 196616 | tf_op jit(solution)/shard_map/ppermute | solution.py:407

commit v3 on v2

--- a/solution.py
+++ b/solution.py
@@ -20,6 +20,7 @@
 MIB = 1 << 20
 VMEM = pl.BlockSpec(memory_space=pltpu.VMEM)
 SMEM = pl.BlockSpec(memory_space=pltpu.SMEM)
+HBM = pl.BlockSpec(memory_space=pltpu.HBM)
 
 
 def granted(mib):
@@ -52,6 +53,7 @@
 MIB = 1 << 20
 VMEM = pl.BlockSpec(memory_space=pltpu.VMEM)
 SMEM = pl.BlockSpec(memory_space=pltpu.SMEM)
+HBM = pl.BlockSpec(memory_space=pltpu.HBM)
 
 
 def granted(mib):
@@ -88,24 +90,34 @@
     return high, mid, (rest - mid).astype(BF16).astype(F32)
 
 
-def pack_kernel(x, extra, out):
+def pack_kernel(x, extra, out, held, sem):
     prompts, seg, width = x.shape
     first = lax.axis_index("sp") // prompts * 2 + SHIFT
+    which = lambda i: lax.rem(first + i, prompts)
+    copies = [
+        pltpu.make_async_copy(x.at[which(i)], out.at[i, pl.ds(0, seg)], sem.at[i])
+        for i in range(prompts)
+    ]
+    copies.append(pltpu.make_async_copy(extra, held, sem.at[prompts]))
+    for copy in reversed(copies):
+        copy.start()
+    copies[-1].wait()
     for i in range(prompts):
-        prompt = lax.rem(first + i, prompts)
-        out[i, :seg, :] = x[prompt]
-        rows = list(three_pieces(extra[pl.ds(prompt, 1), :])) + [jnp.zeros((PAD - 3, width), F32)]
+        rows = list(three_pieces(held[pl.ds(which(i), 1), :])) + [jnp.zeros((PAD - 3, width), F32)]
         out[i, seg:, :] = jnp.concatenate(rows, axis=0).astype(BF16)
+    for copy in copies[:-1]:
+        copy.wait()
 
 
 def packed(layer_input, extra):
     prompts, seg, width = layer_input.shape
     return pl.pallas_call(
         pack_kernel,
-        in_specs=[VMEM, VMEM],
+        in_specs=[HBM, HBM],
         out_specs=VMEM,
         out_shape=jax.ShapeDtypeStruct((prompts, seg + PAD, width), BF16),
-        compiler_params=granted(4),
+        scratch_shapes=[pltpu.VMEM(extra.shape, F32), pltpu.SemaphoreType.DMA((prompts + 1,))],
+        compiler_params=granted(60),
     )(layer_input, extra)
 
 
@@ -168,42 +180,52 @@
         step *= 2
 
 
-def map_kernel(
-    xg, wk, wv, wok, wov, wg, mine, other, acc, gates, keys, low, low_rest, inverse, product, right, solved, maps
-):
+def partner_kernel(xg, first, second, wg, out, gates, *scratch):
+    *scratch, weights, sem = scratch
+    core = lax.axis_index("sp") % 2
+    copies = [
+        pltpu.make_async_copy(first, weights.at[core], sem.at[0]),
+        pltpu.make_async_copy(second, weights.at[1 - core], sem.at[1]),
+    ]
+    for copy in copies:
+        copy.start()
+    x = features(xg)
+    gates[...] = dot1(wg[...], x, NT)
+    for copy in copies:
+        copy.wait()
+    head_map(lax.axis_index("tp") ^ 1, x, xg, weights[0], weights[1], gates, out, *scratch)
+
+
+def own_kernel(xg, w_key, w_value, gates, out, *scratch):
+    head_map(lax.axis_index("tp"), features(xg), xg, w_key[...], w_value[...], gates, out, *scratch)
+
+
+def features(xg):
+    sources, rows, _ = xg.shape
+    return jnp.concatenate([xg[i, : rows - PAD, :] for i in range(sources)], axis=1)
+
+
+def head_map(head, x, xg, w_key, w_value, gates, out, acc, keys, low, low_rest, inverse, product, right, solved, maps):
     sources, rows, width = xg.shape
     rows = rows - PAD
-    blocks = rows // BLOCK
-    units = 2 * blocks
-    me = lax.axis_index("tp")
-    x = jnp.concatenate([xg[i, :rows, :] for i in range(sources)], axis=1)
-    gates[...] = dot1(wg[...], x, NT)
-    acc[0] = dot1(x, jnp.concatenate([wk[...], wv[...]], axis=1))
-    acc[1] = dot1(x, jnp.concatenate([wok[...], wov[...]], axis=1))
+    blocks = units = rows // BLOCK
+    acc[...] = dot1(x, jnp.concatenate([w_key, w_value], axis=1))
 
     row = lax.broadcasted_iota(jnp.int32, (BLOCK, BLOCK), 0)
     col = lax.broadcasted_iota(jnp.int32, (BLOCK, BLOCK), 1)
     upto = (row <= col).astype(F32)
     strict = row > col
-    decays, betas = [], []
-    for which in range(2):
-        head = me if which == 0 else me ^ 1
-        extras = xg[head, rows:, :].astype(F32)
-        extra = extras[0:4] + extras[4:8] + extras[8:12]
-        consts = extras[12:13] + extras[13:14] + extras[14:15]
-        rate, bias = consts[:, 0:1], consts[:, width // 2 : width // 2 + 1]
-        cut = lambda g: jnp.concatenate(
-            [g[:, BLOCK * b : BLOCK * (b + 1)] for b in range(blocks)], axis=0
-        )
-        decay_pre = cut(gates[pl.ds(head, 1), :])
-        beta_pre = cut(gates[pl.ds(sources + head, 1), :])
-        soft = jnp.maximum(decay_pre, 0.0) + jnp.log1p(jnp.exp(-jnp.abs(decay_pre)))
-        decays.append(-rate * soft + extra)
-        betas.append(jax.nn.sigmoid(beta_pre + bias))
-    running = jnp.dot(
-        jnp.concatenate(decays, axis=0), upto, precision=HIGH, preferred_element_type=F32
-    )
-    beta = jnp.concatenate(betas, axis=0)
+    extras = xg[head, rows:, :].astype(F32)
+    extra = extras[0:4] + extras[4:8] + extras[8:12]
+    consts = extras[12:13] + extras[13:14] + extras[14:15]
+    rate, bias = consts[:, 0:1], consts[:, width // 2 : width // 2 + 1]
+    cut = lambda g: jnp.concatenate([g[:, BLOCK * b : BLOCK * (b + 1)] for b in range(blocks)], axis=0)
+    decay_pre = cut(gates[pl.ds(head, 1), :])
+    beta_pre = cut(gates[pl.ds(sources + head, 1), :])
+    soft = jnp.maximum(decay_pre, 0.0) + jnp.log1p(jnp.exp(-jnp.abs(decay_pre)))
+    beta = jax.nn.sigmoid(beta_pre + bias)
+    decay = jnp.concatenate([-rate * soft + extra, jnp.zeros((8 - blocks, BLOCK), F32)], axis=0)
+    running = jnp.dot(decay, upto, precision=HIGH, preferred_element_type=F32)[:units]
     tall = jnp.concatenate([running, beta, jnp.zeros((BLOCK - 2 * units, BLOCK), F32)], axis=0)
     columns = tall.T
     run_col = lambda u: jnp.broadcast_to(columns[:, u : u + 1], (BLOCK, BLOCK))
@@ -211,8 +233,7 @@
     run_row = lambda u: jnp.broadcast_to(running[u : u + 1, :], (BLOCK, BLOCK))
     last = lambda u: jnp.broadcast_to(running[u : u + 1, BLOCK - 1 :], (BLOCK, BLOCK))
     for u in range(units):
-        which, b = divmod(u, blocks)
-        pre = acc[which, BLOCK * b : BLOCK * (b + 1), :]
+        pre = acc[BLOCK * u : BLOCK * (u + 1), :]
         act = pre * jax.nn.sigmoid(pre)
         key, value = act[:, :DK], act[:, DK:]
         key = key * lax.rsqrt(jnp.sum(key * key, axis=1, keepdims=True) + EPS)
@@ -251,7 +272,7 @@
             if 2 * apart < blocks:
                 maps[u] = result
             else:
-                (mine, other)[u // blocks][...] = result
+                out[...] = result
         apart *= 2
 
 
@@ -260,19 +281,16 @@
     return jnp.concatenate([both[:, :DK], both[:, DK:] + later[:, DK:]], axis=1)
 
 
-def local_maps(xg, w_key, w_value, other_key, other_value, gate_rows):
-    _, rows, _ = xg.shape
-    used = rows - PAD
-    units = 2 * (used // BLOCK)
+def head_call(kernel, outs, more, used, specs, *operands):
+    units = used // BLOCK
     shape = jax.ShapeDtypeStruct((DK, DK + DV), F32)
     return pl.pallas_call(
-        map_kernel,
-        in_specs=[VMEM] * 6,
-        out_specs=[VMEM] * 2,
-        out_shape=[shape] * 2,
+        kernel,
+        in_specs=specs,
+        out_specs=[VMEM] * (1 + len(outs)),
+        out_shape=[shape, *outs],
         scratch_shapes=[
-            pltpu.VMEM((2, used, DK + DV), F32),
-            pltpu.VMEM((gate_rows.shape[0], used), F32),
+            pltpu.VMEM((used, DK + DV), F32),
             pltpu.VMEM((units, BLOCK, DK), F32),
             pltpu.VMEM((units, BLOCK, BLOCK), BF16),
             pltpu.VMEM((units, BLOCK, BLOCK), BF16),
@@ -281,9 +299,10 @@
             pltpu.VMEM((units, BLOCK, DK + DV), F32),
             pltpu.VMEM((units, BLOCK, DK + DV), BF16),
             pltpu.VMEM((units, DK, DK + DV), F32),
+            *more,
         ],
-        compiler_params=granted(28),
-    )(xg, w_key, w_value, other_key, other_value, gate_rows)
+        compiler_params=granted(24),
+    )(*operands)
 
 
 def in_order(mine, other, late):
@@ -292,8 +311,26 @@
     return composed(earlier, later)
 
 
+def diagonal():
+    row = lax.broadcasted_iota(jnp.int32, (DK, DK), 0)
+    return row == lax.broadcasted_iota(jnp.int32, (DK, DK), 1)
+
+
 def pair_kernel(mine, other, out):
-    out[...] = in_order(mine[...], other[...], lax.axis_index("tp") % 2 == 1)
+    whole = in_order(mine[...], other[...], lax.axis_index("tp") % 2 == 1)
+    out[:DK, :] = whole.astype(BF16)
+    part = whole[:, :DK]
+    lost = part - part.astype(BF16).astype(F32)
+    lost = jnp.sum(jnp.where(diagonal(), lost, 0.0), axis=0, keepdims=True)
+    lost = jnp.concatenate([lost, jnp.zeros((PAD - 1, DK), F32)], axis=0)
+    out[DK:, :] = jnp.concatenate([lost, jnp.zeros_like(lost)], axis=1).astype(BF16)
+
+
+def widened(sent):
+    whole = sent[:DK, :].astype(F32)
+    lost = sent[DK:, :DK].astype(F32)[:1]
+    part = whole[:, :DK] + jnp.where(diagonal(), jnp.broadcast_to(lost, (DK, DK)), 0.0)
+    return jnp.concatenate([part, whole[:, DK:]], axis=1)
 
 
 def pair_composed(mine, other):
@@ -301,7 +338,7 @@
         pair_kernel,
         in_specs=[VMEM] * 2,
         out_specs=VMEM,
-        out_shape=jax.ShapeDtypeStruct(mine.shape, F32),
+        out_shape=jax.ShapeDtypeStruct((DK + PAD, DK + DV), BF16),
         compiler_params=granted(4),
     )(mine, other)
 
@@ -311,7 +348,7 @@
 
 def couple_kernel(mine, other, keep, give):
     place = lax.axis_index("sp")
-    whole = in_order(mine[...], other[...], place % 2 == 1)
+    whole = in_order(widened(mine[...]), widened(other[...]), place % 2 == 1)
     keep[...] = whole
     core = place % 2
 
@@ -332,7 +369,7 @@
         couple_kernel,
         in_specs=[VMEM] * 2,
         out_specs=[VMEM] * 2,
-        out_shape=[jax.ShapeDtypeStruct(mine.shape, F32), jax.ShapeDtypeStruct((DK, DV), F32)],
+        out_shape=[jax.ShapeDtypeStruct((DK, DK + DV), F32), jax.ShapeDtypeStruct((DK, DV), F32)],
         compiler_params=granted(4),
     )(mine, other)
 
@@ -380,9 +417,11 @@
     sp = lax.axis_size("sp")
     tp = lax.axis_size("tp")
     chunks = sp // prompts
+    place = lax.axis_index("sp")
     pair = [(i, i ^ 1) for i in range(tp)]
-    other_key = lax.ppermute(w_key, "tp", pair)
-    other_value = lax.ppermute(w_value, "tp", pair)
+    picked = jnp.where(place % 2 == 1, w_value, w_key)
+    first = lax.ppermute(picked, "tp", pair)
+    second = lax.ppermute(first, "sp", [(i, i ^ 1) for i in range(sp)])
 
     sent = packed(layer_input, log_decay_extra[:, 0, :])
     groups = [[prompts * t + j for j in range(prompts)] for t in range(chunks)]
@@ -392,8 +431,19 @@
     gathered = lax.all_to_all(parcel, "tp", 0, 0, tiled=True)
 
     gate_rows = w_gates.transpose(0, 2, 1).reshape(2 * tp, -1)
-    mine, theirs = local_maps(gathered, w_key, w_value, other_key, other_value, gate_rows)
+    used = gathered.shape[1] - PAD
+    gate_shape = jax.ShapeDtypeStruct((gate_rows.shape[0], used), F32)
+    held = [pltpu.VMEM((2, *w_key.shape), BF16), pltpu.SemaphoreType.DMA((2,))]
+    theirs, gates = head_call(
+        partner_kernel,
+        [gate_shape],
+        held,
+        used,
+        [VMEM, HBM, HBM, VMEM],
+        *(gathered, first, second, gate_rows),
+    )
     other = lax.ppermute(theirs, "tp", pair)
+    (mine,) = head_call(own_kernel, [], [], used, [VMEM] * 4, gathered, w_key, w_value, gates)
     whole = pair_composed(mine, other)
 
     ways = [

time: 144 us -> 136 us (0.944)
  waiting for transfers between devices: 62.8 us -> 49.7 us
  Pallas kernels: 7.86 us -> 12.5 us
  starting transfers between devices: 39.8 us -> 43.1 us
  blocking collectives: 23.8 us -> 21.7 us
  local copies, waits for them, and re-layouts: 6.65 us -> 5.04 us
    ppermute x2, waiting for transfers between devices: 43.8 us -> 36.1 us  [the longest x1 35.3 us: shards(): first = lax.ppermute(picked, 'tp', pair)]
    pallas_call x2 -> x3, Pallas kernels: 6.42 us -> 11.1 us  [the longest x2 9.39 us: head_call(): pl.pallas_call(kernel, in_specs=specs, out_specs=[VMEM] * (1 + len(outs))...]
    ppermute x1, waiting for transfers between devices: 3.78 us -> 0.35 us  [shards(): other = lax.ppermute(theirs, 'tp', pair)]
    ppermute x1, starting transfers between devices: 3.3 us -> 6.68 us  [shards(): got = lax.ppermute(give, 'sp', [(i, i ^ 2) for i in range(sp)])]
    all_to_all x1, blocking collectives: 23.8 us -> 21.7 us  [shards(): lax.all_to_all(jnp.broadcast_to(partial[None], (sp, 1, DV)), 'sp', 0, 0,...]
    ppermute x1, starting transfers between devices: 13.1 us -> 11 us  [shards(): moved = lax.ppermute(whole, 'sp', ways)]
    ppermute x2, starting transfers between devices: 5.28 us -> 7.33 us  [the longest x1 4.07 us: shards(): second = lax.ppermute(first, 'sp', [(i, i ^ 1) for i in range(sp)])]
    ppermute x1, waiting for transfers between devices: 3.76 us -> 1.92 us  [shards(): moved = lax.ppermute(whole, 'sp', ways)]
  transfers between devices with their start and end apart: 8 -> 8, of which waited for: 7 -> 7; matrix products, arithmetic and copies ran while one was open for 0% -> 0% of each run, Pallas kernels for 0% -> 3%
where the time goes in v3:
time: 136 us; the launch traced here: 135 us
  waiting for transfers between devices  49.7 us (37%)
  starting transfers between devices  43.1 us (32%)
  blocking collectives  21.7 us (16%)
  Pallas kernels  12.5 us (9%)
  local copies, waits for them, and re-layouts  5.04 us (4%)
  between operations  2.11 us (2%)
    ppermute x1, waiting for transfers between devices, shards(): first = lax.ppermute(picked, 'tp', pair)  35.3 us
    all_to_all x1, blocking collectives, shards(): lax.all_to_all(jnp.broadcast_to(partial[None], (sp, 1, DV)), 'sp', 0, 0,...  21.7 us
    ppermute x1, starting transfers between devices, shards(): moved = lax.ppermute(whole, 'sp', ways)  11 us
    all_to_all x1, starting transfers between devices, shards(): lax.all_to_all(sent, 'sp', 0, 0, axis_index_groups=groups, tiled=True)  10.2 us
    pallas_call x2, Pallas kernels, head_call(): pl.pallas_call(kernel, in_specs=specs, out_specs=[VMEM] * (1 + len(outs))...  9.39 us
    all_to_all x1, waiting for transfers between devices, shards(): lax.all_to_all(sent, 'sp', 0, 0, axis_index_groups=groups, tiled=True)  8.06 us
    ppermute x1, starting transfers between devices, shards(): got = lax.ppermute(give, 'sp', [(i, i ^ 2) for i in range(sp)])  6.68 us
    unnamed x20, local copies, waits for them, and re-layouts  5.03 us
  transfers between devices with their start and end apart: 8, of which 7 were waited for; matrix products, arithmetic and copies ran while one was open for 0% of the time, Pallas kernels for 3%

profile of v3, /device:TPU:1, one launch (start us, length us, event | category | flops | bytes accessed | tf_op | source)
XLA Modules:
  0.0 135.1 jit_solution(1027935802634131114)
XLA Ops:
  0.6 1.7 %shard_map.104 = bf16[8,144,128]{2,1,0:T(8,128)(2,1)} custom-call(bf16[8,128,128]{2,1,0:T(8,128)(2,1)} %x.1, f32[8,128]{1,0:T(8,128)} %bitcast.9), custom_call_target="tpu_custom_call" | custom-call | tf_op jit(solution)/shard_map/pallas_call | solution.py:114
  2.3 10.2 %all-to-all-start = ((bf16[8,144,128]{2,1,0:T(8,128)(2,1)}), bf16[8,144,128]{2,1,0:T(8,128)(2,1)S(1)}, u32[]{:S(2)}, u32[]{:S(2)}) async-start(bf16[8,144,128]{2,1,0:T(8,128)(2,1)} %shard_map.104), calls=%async_computation | async-start | bytes 589824 | tf_op jit(solution)/shard_map/all_to_all | solution.py:428
  13.8 8.1 %all-to-all-done.here = bf16[8,144,128]{2,1,0:T(8,128)(2,1)S(1)} async-done(((bf16[8,144,128]{2,1,0:T(8,128)(2,1)}), bf16[8,144,128]{2,1,0:T(8,128)(2,1)S(1)}, u32[]{:S(2)}, u32[]{:S(2)}) %all-to-all-start) | async-done | bytes 294944 | tf_op jit(solution)/shard_map/all_to_all | solution.py:428
  22.1 1.3 copy-done
  23.5 4.1 %all-to-all-start.1 = ((bf16[16,528,128]{2,1,0:T(8,128)(2,1)}), bf16[16,528,128]{2,1,0:T(8,128)(2,1)S(1)}, u32[]{:S(2)}, u32[]{:S(2)}) async-start(bf16[16,528,128]{2,1,0:T(8,128)(2,1)} %copy-done), calls=%async_computation.1 | async-start | bytes 4325376 | tf_op jit(solution)/shard_map/all_to_all | solution.py:431
  27.7 3.3 %collective-permute-start = (bf16[2048,128]{1,0:T(8,128)(2,1)S(1)}, bf16[2048,128]{1,0:T(8,128)(2,1)S(1)}, u32[]{:S(2)}, u32[]{:S(2)}) collective-permute-start(bf16[2048,128]{1,0:T(8,128)(2,1)S(1)} %broadcast_select_fusion), channel_id=1, source_target_pairs={{0,1},{1,0},{2,3},{3,2},{4,5},{5,4},{6,7},{7,6},{8,9},{9,8},{10,11... | collective-permute-start | bytes 1572872 | tf_op jit(solution)/shard_map/ppermute | solution.py:423
  31.0 35.3 %collective-permute-done.first = bf16[2048,128]{1,0:T(8,128)(2,1)S(1)} collective-permute-done((bf16[2048,128]{1,0:T(8,128)(2,1)S(1)}, bf16[2048,128]{1,0:T(8,128)(2,1)S(1)}, u32[]{:S(2)}, u32[]{:S(2)}) %collective-permute-start) | collective-permute-done | bytes 524320 | tf_op jit(solution)/shard_map/ppermute | solution.py:423
  66.3 4.1 %collective-permute-start.1 = (bf16[2048,128]{1,0:T(8,128)(2,1)S(1)}, bf16[2048,128]{1,0:T(8,128)(2,1)S(1)}, u32[]{:S(2)}, u32[]{:S(2)}) collective-permute-start(bf16[2048,128]{1,0:T(8,128)(2,1)S(1)} %collective-permute-done.first), channel_id=1, source_target_pairs={{0,16},{16,0},{32,48},{48,32},{64,80},{80,64},{96,112},{112,96},{1... | collective-permute-start | bytes 1572872 | tf_op jit(solution)/shard_map/ppermute | solution.py:424
  70.4 0.8 copy-done.3
  71.2 0.7 collective-permute-done.1.second
  71.9 0.8 copy-done.5
  72.7 1.0 copy-done.4
  73.8 1.0 copy-done.6
  74.8 5.1 %shard_map.106 = (f32[128,256]{1,0:T(8,128)S(1)}, f32[32,512]{1,0:T(8,128)S(1)}) custom-call(bf16[16,528,128]{2,1,0:T(8,128)(2,1)S(1)} %all-to-all-done.1.xg, bf16[2048,128]{1,0:T(8,128)(2,1)S(1)} %copy-done.4, bf16[2048,128]{1,0:T(8,128)(2,1)S(1)} %copy-done.6, bf16[32,2048]{1,0:T(8,128)(2,1)S(1)} %bitcast.6), custom_call_target="tpu_custom_call" | custom-call | tf_op jit(solution)/shard_map/pallas_call | solution.py:287
  79.9 1.9 %collective-permute-start.2 = (f32[128,256]{1,0:T(8,128)S(1)}, f32[128,256]{1,0:T(8,128)S(1)}, u32[]{:S(2)}, u32[]{:S(2)}) collective-permute-start(f32[128,256]{1,0:T(8,128)S(1)} %get-tuple-element.9), channel_id=1, source_target_pairs={{0,1},{1,0},{2,3},{3,2},{4,5},{5,4},{6,7},{7,6},{8,9},{9,8},{10,11... | collective-permute-start | bytes 393224 | tf_op jit(solution)/shard_map/ppermute | solution.py:445
  81.9 4.3 %shard_map.107.mine = f32[128,256]{1,0:T(8,128)S(1)} custom-call(bf16[16,528,128]{2,1,0:T(8,128)(2,1)S(1)} %all-to-all-done.1.xg, bf16[2048,128]{1,0:T(8,128)(2,1)S(1)} %copy-done.1, bf16[2048,128]{1,0:T(8,128)(2,1)S(1)} %copy-done.2, f32[32,512]{1,0:T(8,128)S(1)} %get-tuple-element.8.gates), custom_call_target="tpu_custom_call" | custom-call | tf_op jit(solution)/shard_map/pallas_call | solution.py:287
  86.7 11.0 %collective-permute-start.3 = (bf16[144,256]{1,0:T(8,128)(2,1)S(1)}, bf16[144,256]{1,0:T(8,128)(2,1)S(1)}, u32[]{:S(2)}, u32[]{:S(2)}) collective-permute-start(bf16[144,256]{1,0:T(8,128)(2,1)S(1)} %shard_map.108), channel_id=1, source_target_pairs={{0,320},{16,384},{32,448},{48,0},{64,64},{80,128},{96,192},{112,25... | collective-permute-start | bytes 221192 | tf_op jit(solution)/shard_map/ppermute | solution.py:454
  97.7 1.9 %collective-permute-done.3.mine = bf16[144,256]{1,0:T(8,128)(2,1)S(1)} collective-permute-done((bf16[144,256]{1,0:T(8,128)(2,1)S(1)}, bf16[144,256]{1,0:T(8,128)(2,1)S(1)}, u32[]{:S(2)}, u32[]{:S(2)}) %collective-permute-start.3) | collective-permute-done | bytes 73760 | tf_op jit(solution)/shard_map/ppermute | solution.py:454
  99.7 1.9 %collective-permute-start.4 = (bf16[144,256]{1,0:T(8,128)(2,1)S(1)}, bf16[144,256]{1,0:T(8,128)(2,1)S(1)}, u32[]{:S(2)}, u32[]{:S(2)}) collective-permute-start(bf16[144,256]{1,0:T(8,128)(2,1)S(1)} %collective-permute-done.3.mine), channel_id=1, source_target_pairs={{0,16},{16,0},{32,48},{48,32},{64,80},{80,64},{96,112},{112,96},{1... | collective-permute-start | bytes 221192 | tf_op jit(solution)/shard_map/ppermute | solution.py:455
  101.6 1.2 collective-permute-done.4.other
  103.0 6.7 %collective-permute-start.5 = (f32[128,128]{1,0:T(8,128)S(1)}, f32[128,128]{1,0:T(8,128)S(1)}, u32[]{:S(2)}, u32[]{:S(2)}) collective-permute-start(f32[128,128]{1,0:T(8,128)S(1)} %get-tuple-element.11), channel_id=1, source_target_pairs={{0,32},{16,48},{32,0},{48,16},{64,96},{80,112},{96,64},{112,80},{1... | collective-permute-start | bytes 196616 | tf_op jit(solution)/shard_map/ppermute | solution.py:457
  109.7 2.1 %collective-permute-done.5.got = f32[128,128]{1,0:T(8,128)S(1)} collective-permute-done((f32[128,128]{1,0:T(8,128)S(1)}, f32[128,128]{1,0:T(8,128)S(1)}, u32[]{:S(2)}, u32[]{:S(2)}) %collective-permute-start.5) | collective-permute-done | bytes 65568 | tf_op jit(solution)/shard_map/ppermute | solution.py:457
  111.8 0.8 shard_map.110
  112.6 21.7 %all_to_all.15 = f32[32,1,128]{2,1,0:T(1,128)S(1)} all-to-all(f32[32,1,128]{2,1,0:T(1,128)S(1)} %broadcast_in_dim.5), channel_id=1, replica_groups=mesh['sp'=32,'tp'=16] {'sp'}, dimensions={0} | all-to-all | bytes 32768 | tf_op jit(solution)/shard_map/all_to_all | solution.py:460
  (26 shorter events, 2.0 us)
Async XLA Ops:
  2.3 19.5 %all-to-all-start = ((bf16[8,144,128]{2,1,0:T(8,128)(2,1)}), bf16[8,144,128]{2,1,0:T(8,128)(2,1)S(1)}, u32[]{:S(2)}, u32[]{:S(2)}) async-start(bf16[8,144,128]{2,1,0:T(8,128)(2,1)} %shard_map.104), calls=%async_computation | async-start | bytes 589824 | tf_op jit(solution)/shard_map/all_to_all | solution.py:428
  22.1 1.4 %copy-start = (bf16[16,528,128]{2,1,0:T(8,128)(2,1)}, bf16[16,528,128]{2,1,0:T(8,128)(2,1)S(1)}, u32[]{:S(2)}) copy-start(bf16[16,528,128]{2,1,0:T(8,128)(2,1)S(1)} %shard_map.105) | copy-start | bytes 6488068
  23.5 4.1 %copy-start.1 = (bf16[2048,128]{1,0:T(8,128)(2,1)S(1)}, bf16[2048,128]{1,0:T(8,128)(2,1)}, u32[]{:S(2)}) copy-start(bf16[2048,128]{1,0:T(8,128)(2,1)} %w_key.1) | copy-start | bytes 1572868
  23.5 4.1 %copy-start.2 = (bf16[2048,128]{1,0:T(8,128)(2,1)S(1)}, bf16[2048,128]{1,0:T(8,128)(2,1)}, u32[]{:S(2)}) copy-start(bf16[2048,128]{1,0:T(8,128)(2,1)} %w_value.1) | copy-start | bytes 1572868
  23.5 49.2 %copy-start.7 = (bf16[2,2048,16]{1,2,0:T(8,128)(2,1)S(1)}, bf16[2,2048,16]{1,2,0:T(8,128)(2,1)}, u32[]{:S(2)}) copy-start(bf16[2,2048,16]{1,2,0:T(8,128)(2,1)} %param.12) | copy-start | bytes 393220
  23.5 49.2 %all-to-all-start.1 = ((bf16[16,528,128]{2,1,0:T(8,128)(2,1)}), bf16[16,528,128]{2,1,0:T(8,128)(2,1)S(1)}, u32[]{:S(2)}, u32[]{:S(2)}) async-start(bf16[16,528,128]{2,1,0:T(8,128)(2,1)} %copy-done), calls=%async_computation.1 | async-start | bytes 4325376 | tf_op jit(solution)/shard_map/all_to_all | solution.py:431
  27.7 38.6 %collective-permute-start = (bf16[2048,128]{1,0:T(8,128)(2,1)S(1)}, bf16[2048,128]{1,0:T(8,128)(2,1)S(1)}, u32[]{:S(2)}, u32[]{:S(2)}) collective-permute-start(bf16[2048,128]{1,0:T(8,128)(2,1)S(1)} %broadcast_select_fusion), channel_id=1, source_target_pairs={{0,1},{1,0},{2,3},{3,2},{4,5},{5,4},{6,7},{7,6},{8,9},{9,8},{10,11... | collective-permute-start | bytes 1572872 | tf_op jit(solution)/shard_map/ppermute | solution.py:423
  66.3 5.6 %collective-permute-start.1 = (bf16[2048,128]{1,0:T(8,128)(2,1)S(1)}, bf16[2048,128]{1,0:T(8,128)(2,1)S(1)}, u32[]{:S(2)}, u32[]{:S(2)}) collective-permute-start(bf16[2048,128]{1,0:T(8,128)(2,1)S(1)} %collective-permute-done.first), channel_id=1, source_target_pairs={{0,16},{16,0},{32,48},{48,32},{64,80},{80,64},{96,112},{112,96},{1... | collective-permute-start | bytes 1572872 | tf_op jit(solution)/shard_map/ppermute | solution.py:424
  70.4 0.8 copy-start.3
  71.9 0.8 copy-start.5
  72.7 1.0 copy-start.4
  73.7 1.0 copy-start.6
  79.9 31.9 %copy-start.8 = (bf16[8,128]{1,0:T(8,128)(2,1)S(1)}, bf16[8,128]{1,0:T(8,128)(2,1)}, u32[]{:S(2)}) copy-start(bf16[8,128]{1,0:T(8,128)(2,1)} %query.1) | copy-start | bytes 6148
  79.9 54.5 %copy-start.9 = (f32[128]{0:T(128)S(1)}, f32[128]{0:T(128)}, u32[]{:S(2)}) copy-start(f32[128]{0:T(128)} %param.17) | copy-start | bytes 1540
  79.9 6.6 %collective-permute-start.2 = (f32[128,256]{1,0:T(8,128)S(1)}, f32[128,256]{1,0:T(8,128)S(1)}, u32[]{:S(2)}, u32[]{:S(2)}) collective-permute-start(f32[128,256]{1,0:T(8,128)S(1)} %get-tuple-element.9), channel_id=1, source_target_pairs={{0,1},{1,0},{2,3},{3,2},{4,5},{5,4},{6,7},{7,6},{8,9},{9,8},{10,11... | collective-permute-start | bytes 393224 | tf_op jit(solution)/shard_map/ppermute | solution.py:445
  86.7 13.0 %collective-permute-start.3 = (bf16[144,256]{1,0:T(8,128)(2,1)S(1)}, bf16[144,256]{1,0:T(8,128)(2,1)S(1)}, u32[]{:S(2)}, u32[]{:S(2)}) collective-permute-start(bf16[144,256]{1,0:T(8,128)(2,1)S(1)} %shard_map.108), channel_id=1, source_target_pairs={{0,320},{16,384},{32,448},{48,0},{64,64},{80,128},{96,192},{112,25... | collective-permute-start | bytes 221192 | tf_op jit(solution)/shard_map/ppermute | solution.py:454
  99.7 3.1 %collective-permute-start.4 = (bf16[144,256]{1,0:T(8,128)(2,1)S(1)}, bf16[144,256]{1,0:T(8,128)(2,1)S(1)}, u32[]{:S(2)}, u32[]{:S(2)}) collective-permute-start(bf16[144,256]{1,0:T(8,128)(2,1)S(1)} %collective-permute-done.3.mine), channel_id=1, source_target_pairs={{0,16},{16,0},{32,48},{48,32},{64,80},{80,64},{96,112},{112,96},{1... | collective-permute-start | bytes 221192 | tf_op jit(solution)/shard_map/ppermute | solution.py:455
  103.0 8.8 %collective-permute-start.5 = (f32[128,128]{1,0:T(8,128)S(1)}, f32[128,128]{1,0:T(8,128)S(1)}, u32[]{:S(2)}, u32[]{:S(2)}) collective-permute-start(f32[128,128]{1,0:T(8,128)S(1)} %get-tuple-element.11), channel_id=1, source_target_pairs={{0,32},{16,48},{32,0},{48,16},{64,96},{80,112},{96,64},{112,80},{1... | collective-permute-start | bytes 196616 | tf_op jit(solution)/shard_map/ppermute | solution.py:457

commit v4 on v3

--- a/solution.py
+++ b/solution.py
@@ -14,6 +14,7 @@
 F32 = jnp.float32
 BF16 = jnp.bfloat16
 PAD = 16
+GRANT = 24
 SHIFT = 5
 
 
@@ -150,14 +151,14 @@
     )(here, rate, bias)
 
 
-def invert_unit_lower(low, inverse, product, row, col):
-    units, size, _ = low.shape
+def invert_unit_lower(units, row, col):
+    size = BLOCK
     step = 1
     while step < size:
         merge = ((row // (2 * step)) == (col // (2 * step))) & ((row // step) != (col // step))
         if step == 1:
             eye = (row == col).astype(F32)
-            for u in range(units):
+            for low, inverse, _, u in units:
                 part = jnp.where(merge, low[u].astype(F32), 0.0)
                 inverse[u] = (eye - part).astype(BF16)
         else:
@@ -166,13 +167,13 @@
             else:
                 lower_rows = [(at, step) for at in range(step, size, 2 * step)]
             rows = sum(length for _, length in lower_rows)
-            take = lambda u: jnp.concatenate([inverse[u, at : at + n, :] for at, n in lower_rows], axis=0)
-            for u in range(units):
+            take = lambda ref, u: jnp.concatenate([ref[u, at : at + n, :] for at, n in lower_rows], axis=0)
+            for low, inverse, product, u in units:
                 part = jnp.where(merge, low[u].astype(F32), 0.0).astype(BF16)
-                product[u, :rows, :] = dot1(take(u), part).astype(BF16)
-            for u in range(units):
+                product[u, :rows, :] = dot1(take(inverse, u), part).astype(BF16)
+            for _, inverse, product, u in units:
                 fill = dot1(product[u, :rows, :], inverse[u])
-                fill = (take(u).astype(F32) - fill).astype(BF16)
+                fill = (take(inverse, u).astype(F32) - fill).astype(BF16)
                 done = 0
                 for at, n in lower_rows:
                     inverse[u, at : at + n, :] = fill[done : done + n]
@@ -180,8 +181,14 @@
         step *= 2
 
 
-def partner_kernel(xg, first, second, wg, out, gates, *scratch):
-    *scratch, weights, sem = scratch
+def squares():
+    row = lax.broadcasted_iota(jnp.int32, (BLOCK, BLOCK), 0)
+    return row, lax.broadcasted_iota(jnp.int32, (BLOCK, BLOCK), 1)
+
+
+def first_kernel(xg, wk, wv, first, second, wg, out, *refs):
+    own, refs = refs[:6], refs[6:]
+    theirs, (acc, gates, product, solved, maps, weights, sem) = refs[:6], refs[6:]
     core = lax.axis_index("sp") % 2
     copies = [
         pltpu.make_async_copy(first, weights.at[core], sem.at[0]),
@@ -189,85 +196,90 @@
     ]
     for copy in copies:
         copy.start()
-    x = features(xg)
+    sources, rows, width = xg.shape
+    rows = rows - PAD
+    blocks = rows // BLOCK
+    x = jnp.concatenate([xg[i, :rows, :] for i in range(sources)], axis=1)
     gates[...] = dot1(wg[...], x, NT)
+    acc[0] = dot1(x, jnp.concatenate([wk[...], wv[...]], axis=1))
     for copy in copies:
         copy.wait()
-    head_map(lax.axis_index("tp") ^ 1, x, xg, weights[0], weights[1], gates, out, *scratch)
-
-
-def own_kernel(xg, w_key, w_value, gates, out, *scratch):
-    head_map(lax.axis_index("tp"), features(xg), xg, w_key[...], w_value[...], gates, out, *scratch)
-
-
-def features(xg):
-    sources, rows, _ = xg.shape
-    return jnp.concatenate([xg[i, : rows - PAD, :] for i in range(sources)], axis=1)
-
-
-def head_map(head, x, xg, w_key, w_value, gates, out, acc, keys, low, low_rest, inverse, product, right, solved, maps):
-    sources, rows, width = xg.shape
-    rows = rows - PAD
-    blocks = units = rows // BLOCK
-    acc[...] = dot1(x, jnp.concatenate([w_key, w_value], axis=1))
-
-    row = lax.broadcasted_iota(jnp.int32, (BLOCK, BLOCK), 0)
-    col = lax.broadcasted_iota(jnp.int32, (BLOCK, BLOCK), 1)
+    acc[1] = dot1(x, jnp.concatenate([weights[0], weights[1]], axis=1))
+
+    row, col = squares()
+    strict = row > col
     upto = (row <= col).astype(F32)
-    strict = row > col
-    extras = xg[head, rows:, :].astype(F32)
-    extra = extras[0:4] + extras[4:8] + extras[8:12]
-    consts = extras[12:13] + extras[13:14] + extras[14:15]
-    rate, bias = consts[:, 0:1], consts[:, width // 2 : width // 2 + 1]
+    me = lax.axis_index("tp")
     cut = lambda g: jnp.concatenate([g[:, BLOCK * b : BLOCK * (b + 1)] for b in range(blocks)], axis=0)
-    decay_pre = cut(gates[pl.ds(head, 1), :])
-    beta_pre = cut(gates[pl.ds(sources + head, 1), :])
-    soft = jnp.maximum(decay_pre, 0.0) + jnp.log1p(jnp.exp(-jnp.abs(decay_pre)))
-    beta = jax.nn.sigmoid(beta_pre + bias)
-    decay = jnp.concatenate([-rate * soft + extra, jnp.zeros((8 - blocks, BLOCK), F32)], axis=0)
-    running = jnp.dot(decay, upto, precision=HIGH, preferred_element_type=F32)[:units]
-    tall = jnp.concatenate([running, beta, jnp.zeros((BLOCK - 2 * units, BLOCK), F32)], axis=0)
-    columns = tall.T
+    decays, betas = [], []
+    for head in (me, me ^ 1):
+        extras = xg[head, rows:, :].astype(F32)
+        extra = extras[0:4] + extras[4:8] + extras[8:12]
+        consts = extras[12:13] + extras[13:14] + extras[14:15]
+        rate, bias = consts[:, 0:1], consts[:, width // 2 : width // 2 + 1]
+        decay_pre = cut(gates[pl.ds(head, 1), :])
+        beta_pre = cut(gates[pl.ds(sources + head, 1), :])
+        soft = jnp.maximum(decay_pre, 0.0) + jnp.log1p(jnp.exp(-jnp.abs(decay_pre)))
+        decays.append(-rate * soft + extra)
+        betas.append(jax.nn.sigmoid(beta_pre + bias))
+    running = jnp.dot(jnp.concatenate(decays, axis=0), upto, precision=HIGH, preferred_element_type=F32)
+    count = 2 * blocks
+    fill = jnp.zeros((BLOCK - 2 * count, BLOCK), F32)
+    columns = jnp.concatenate([running, jnp.concatenate(betas, axis=0), fill], axis=0).T
     run_col = lambda u: jnp.broadcast_to(columns[:, u : u + 1], (BLOCK, BLOCK))
-    beta_col = lambda u: jnp.broadcast_to(columns[:, units + u : units + u + 1], (BLOCK, BLOCK))
-    run_row = lambda u: jnp.broadcast_to(running[u : u + 1, :], (BLOCK, BLOCK))
-    last = lambda u: jnp.broadcast_to(running[u : u + 1, BLOCK - 1 :], (BLOCK, BLOCK))
-    for u in range(units):
-        pre = acc[BLOCK * u : BLOCK * (u + 1), :]
+    beta_col = lambda u: jnp.broadcast_to(columns[:, count + u : count + u + 1], (BLOCK, BLOCK))
+    last = lambda u: jnp.broadcast_to(running[u : u + 1, BLOCK - 1 :], (1, BLOCK))
+    units = [(refs, which * blocks + b, b) for which, refs in enumerate((own, theirs)) for b in range(blocks)]
+    for (late, low, rest, inverse, right, total), u, b in units:
+        which = u // blocks
+        pre = acc[which, BLOCK * b : BLOCK * (b + 1), :]
         act = pre * jax.nn.sigmoid(pre)
         key, value = act[:, :DK], act[:, DK:]
         key = key * lax.rsqrt(jnp.sum(key * key, axis=1, keepdims=True) + EPS)
-        keys[u] = key
-        strength = beta_col(u)
-        right[u, :, :DK] = key * (strength * jnp.exp(run_col(u)))
-        right[u, :, DK:] = value * strength
-    for u in range(units):
-        key = keys[u]
+        late[b] = key
+        right[b, :, :DK] = key * (beta_col(u) * jnp.exp(run_col(u)))
+        right[b, :, DK:] = value * beta_col(u)
+        total[b : b + 1, :] = jnp.exp(last(u))
+    for (late, low, rest, inverse, right, total), u, b in units:
+        key = late[b]
         gram = dot3(key, key, NT)
-        weights = jnp.exp(jnp.where(strict, run_col(u) - run_row(u), 0.0))
-        high, rest = halves(jnp.where(strict, gram * beta_col(u) * weights, 0.0))
-        low[u] = high
-        low_rest[u] = rest
-    invert_unit_lower(low, inverse, product, row, col)
-    for u in range(units):
+        run_row = jnp.broadcast_to(running[u : u + 1, :], (BLOCK, BLOCK))
+        weight = jnp.exp(jnp.where(strict, run_col(u) - run_row, 0.0))
+        high, lower = halves(jnp.where(strict, gram * beta_col(u) * weight, 0.0))
+        low[b] = high
+        rest[b] = lower
+        late[b] = key * jnp.exp(jnp.broadcast_to(last(u), (BLOCK, BLOCK)) - run_col(u))
+    invert_unit_lower(
+        [(refs[1], refs[3], product.at[u // blocks], b) for refs, u, b in units], row, col
+    )
+    finish(theirs, out, solved, maps)
+
+
+def second_kernel(late, low, rest, inverse, right, total, out, solved, maps, held):
+    held[...] = right[...]
+    finish((late, low, rest, inverse, held, total), out, solved, maps)
+
+
+def finish(refs, out, solved, maps):
+    late, low, rest, inverse, right, total = refs
+    row, col = squares()
+    blocks = maps.shape[0]
+    for u in range(blocks):
         solved[u] = dot1(inverse[u], right[u].astype(BF16)).astype(BF16)
-    for u in range(units):
+    for u in range(blocks):
         first = solved[u]
-        taken = dot1(
-            jnp.concatenate([low[u], low_rest[u]], axis=1), jnp.concatenate([first, first], axis=0)
-        )
+        taken = dot1(jnp.concatenate([low[u], rest[u]], axis=1), jnp.concatenate([first, first], axis=0))
         right[u] = right[u] - first.astype(F32) - taken
-    for u in range(units):
+    for u in range(blocks):
         right[u] = solved[u].astype(F32) + dot1(inverse[u], right[u].astype(BF16))
-    for u in range(units):
-        late = keys[u] * jnp.exp(last(u) - run_col(u))
-        made = dot3(late.T, right[u])
-        keep = jnp.where(row == col, jnp.exp(last(u)), 0.0)
+    for u in range(blocks):
+        made = dot3(late[u].T, right[u])
+        keep = jnp.where(row == col, jnp.broadcast_to(total[u : u + 1, :], (BLOCK, BLOCK)), 0.0)
         maps[u, :, :DK] = keep - made[:, :DK]
         maps[u, :, DK:] = made[:, DK:]
     apart = 1
     while apart < blocks:
-        for u in range(0, units, 2 * apart):
+        for u in range(0, blocks, 2 * apart):
             result = composed(maps[u], maps[u + apart])
             if 2 * apart < blocks:
                 maps[u] = result
@@ -281,28 +293,50 @@
     return jnp.concatenate([both[:, :DK], both[:, DK:] + later[:, DK:]], axis=1)
 
 
-def head_call(kernel, outs, more, used, specs, *operands):
-    units = used // BLOCK
-    shape = jax.ShapeDtypeStruct((DK, DK + DV), F32)
-    return pl.pallas_call(
-        kernel,
-        in_specs=specs,
-        out_specs=[VMEM] * (1 + len(outs)),
-        out_shape=[shape, *outs],
+MAP = jax.ShapeDtypeStruct((DK, DK + DV), F32)
+
+
+def block_arrays(blocks):
+    wide, square = (blocks, BLOCK, DK + DV), (blocks, BLOCK, BLOCK)
+    return [(square, F32), (square, BF16), (square, BF16), (square, BF16), (wide, F32), ((8, BLOCK), F32)]
+
+
+def map_scratch(blocks):
+    return [pltpu.VMEM((blocks, BLOCK, DK + DV), BF16), pltpu.VMEM((blocks, DK, DK + DV), F32)]
+
+
+def partner_map(xg, w_key, w_value, first, second, gate_rows):
+    used = xg.shape[1] - PAD
+    blocks = used // BLOCK
+    kept = block_arrays(blocks)
+    return pl.pallas_call(
+        first_kernel,
+        in_specs=[VMEM, VMEM, VMEM, HBM, HBM, VMEM],
+        out_specs=[VMEM] * (1 + len(kept)),
+        out_shape=[MAP] + [jax.ShapeDtypeStruct(*a) for a in kept],
         scratch_shapes=[
-            pltpu.VMEM((used, DK + DV), F32),
-            pltpu.VMEM((units, BLOCK, DK), F32),
-            pltpu.VMEM((units, BLOCK, BLOCK), BF16),
-            pltpu.VMEM((units, BLOCK, BLOCK), BF16),
-            pltpu.VMEM((units, BLOCK, BLOCK), BF16),
-            pltpu.VMEM((units, BLOCK, BLOCK), BF16),
-            pltpu.VMEM((units, BLOCK, DK + DV), F32),
-            pltpu.VMEM((units, BLOCK, DK + DV), BF16),
-            pltpu.VMEM((units, DK, DK + DV), F32),
-            *more,
+            *[pltpu.VMEM(*a) for a in kept],
+            pltpu.VMEM((2, used, DK + DV), F32),
+            pltpu.VMEM((gate_rows.shape[0], used), F32),
+            pltpu.VMEM((2, blocks, BLOCK, BLOCK), BF16),
+            *map_scratch(blocks),
+            pltpu.VMEM((2, *w_key.shape), BF16),
+            pltpu.SemaphoreType.DMA((2,)),
         ],
-        compiler_params=granted(24),
-    )(*operands)
+        compiler_params=granted(GRANT),
+    )(xg, w_key, w_value, first, second, gate_rows)
+
+
+def own_map(*arrays):
+    blocks = arrays[0].shape[0]
+    return pl.pallas_call(
+        second_kernel,
+        in_specs=[VMEM] * len(arrays),
+        out_specs=VMEM,
+        out_shape=MAP,
+        scratch_shapes=[*map_scratch(blocks), pltpu.VMEM((blocks, BLOCK, DK + DV), F32)],
+        compiler_params=granted(8),
+    )(*arrays)
 
 
 def in_order(mine, other, late):
@@ -431,19 +465,9 @@
     gathered = lax.all_to_all(parcel, "tp", 0, 0, tiled=True)
 
     gate_rows = w_gates.transpose(0, 2, 1).reshape(2 * tp, -1)
-    used = gathered.shape[1] - PAD
-    gate_shape = jax.ShapeDtypeStruct((gate_rows.shape[0], used), F32)
-    held = [pltpu.VMEM((2, *w_key.shape), BF16), pltpu.SemaphoreType.DMA((2,))]
-    theirs, gates = head_call(
-        partner_kernel,
-        [gate_shape],
-        held,
-        used,
-        [VMEM, HBM, HBM, VMEM],
-        *(gathered, first, second, gate_rows),
-    )
+    theirs, *kept = partner_map(gathered, w_key, w_value, first, second, gate_rows)
     other = lax.ppermute(theirs, "tp", pair)
-    (mine,) = head_call(own_kernel, [], [], used, [VMEM] * 4, gathered, w_key, w_value, gates)
+    mine = own_map(*kept)
     whole = pair_composed(mine, other)
 
     ways = [

time: 136 us -> 137 us (level)
  waiting for transfers between devices: 49.7 us -> 52.9 us
  Pallas kernels: 12.5 us -> 10.7 us
    ppermute x1, waiting for transfers between devices: 0.35 us -> 3.49 us  [shards(): other = lax.ppermute(theirs, 'tp', pair)]
    pallas_call x2, Pallas kernels: 9.39 us -> 7.56 us  [the longest x1 6.41 us: partner_map(): pl.pallas_call(first_kernel, in_specs=[VMEM, VMEM, VMEM, HBM, HBM, VMEM],...]
  transfers between devices with their start and end apart: 8 -> 8, of which waited for: 7 -> 7; matrix products, arithmetic and copies ran while one was open for 0% -> 0% of each run, Pallas kernels for 3% -> 1%
where the time goes in v4:
time: 137 us; the launch traced here: 136 us
  waiting for transfers between devices  52.9 us (39%)
  starting transfers between devices  43.1 us (31%)
  blocking collectives  21.7 us (16%)
  Pallas kernels  10.7 us (8%)
  local copies, waits for them, and re-layouts  5.03 us (4%)
  between operations  2.1 us (2%)
    ppermute x1, waiting for transfers between devices, shards(): first = lax.ppermute(picked, 'tp', pair)  35.3 us
    all_to_all x1, blocking collectives, shards(): lax.all_to_all(jnp.broadcast_to(partial[None], (sp, 1, DV)), 'sp', 0, 0,...  21.7 us
    ppermute x1, starting transfers between devices, shards(): moved = lax.ppermute(whole, 'sp', ways)  11 us
    all_to_all x1, starting transfers between devices, shards(): lax.all_to_all(sent, 'sp', 0, 0, axis_index_groups=groups, tiled=True)  10.2 us
    all_to_all x1, waiting for transfers between devices, shards(): lax.all_to_all(sent, 'sp', 0, 0, axis_index_groups=groups, tiled=True)  8.06 us
    ppermute x1, starting transfers between devices, shards(): got = lax.ppermute(give, 'sp', [(i, i ^ 2) for i in range(sp)])  6.68 us
    pallas_call x1, Pallas kernels, partner_map(): pl.pallas_call(first_kernel, in_specs=[VMEM, VMEM, VMEM, HBM, HBM, VMEM],...  6.41 us
    unnamed x20, local copies, waits for them, and re-layouts  5.02 us
  transfers between devices with their start and end apart: 8, of which 7 were waited for; matrix products, arithmetic and copies ran while one was open for 0% of the time, Pallas kernels for 1%

profile of v4, /device:TPU:1, one launch (start us, length us, event | category | flops | bytes accessed | tf_op | source)
XLA Modules:
  0.0 136.3 jit_solution(5878154975546965251)
XLA Ops:
  0.6 1.7 %shard_map.104 = bf16[8,144,128]{2,1,0:T(8,128)(2,1)} custom-call(bf16[8,128,128]{2,1,0:T(8,128)(2,1)} %x.1, f32[8,128]{1,0:T(8,128)} %bitcast.9), custom_call_target="tpu_custom_call" | custom-call | tf_op jit(solution)/shard_map/pallas_call | solution.py:115
  2.3 10.2 %all-to-all-start = ((bf16[8,144,128]{2,1,0:T(8,128)(2,1)}), bf16[8,144,128]{2,1,0:T(8,128)(2,1)S(1)}, u32[]{:S(2)}, u32[]{:S(2)}) async-start(bf16[8,144,128]{2,1,0:T(8,128)(2,1)} %shard_map.104), calls=%async_computation | async-start | bytes 589824 | tf_op jit(solution)/shard_map/all_to_all | solution.py:462
  13.8 8.1 %all-to-all-done.here = bf16[8,144,128]{2,1,0:T(8,128)(2,1)S(1)} async-done(((bf16[8,144,128]{2,1,0:T(8,128)(2,1)}), bf16[8,144,128]{2,1,0:T(8,128)(2,1)S(1)}, u32[]{:S(2)}, u32[]{:S(2)}) %all-to-all-start) | async-done | bytes 294944 | tf_op jit(solution)/shard_map/all_to_all | solution.py:462
  22.1 1.3 copy-done
  23.5 4.1 %all-to-all-start.1 = ((bf16[16,528,128]{2,1,0:T(8,128)(2,1)}), bf16[16,528,128]{2,1,0:T(8,128)(2,1)S(1)}, u32[]{:S(2)}, u32[]{:S(2)}) async-start(bf16[16,528,128]{2,1,0:T(8,128)(2,1)} %copy-done), calls=%async_computation.1 | async-start | bytes 4325376 | tf_op jit(solution)/shard_map/all_to_all | solution.py:465
  27.7 3.3 %collective-permute-start = (bf16[2048,128]{1,0:T(8,128)(2,1)S(1)}, bf16[2048,128]{1,0:T(8,128)(2,1)S(1)}, u32[]{:S(2)}, u32[]{:S(2)}) collective-permute-start(bf16[2048,128]{1,0:T(8,128)(2,1)S(1)} %broadcast_select_fusion), channel_id=1, source_target_pairs={{0,1},{1,0},{2,3},{3,2},{4,5},{5,4},{6,7},{7,6},{8,9},{9,8},{10,11... | collective-permute-start | bytes 1572872 | tf_op jit(solution)/shard_map/ppermute | solution.py:457
  31.0 35.3 %collective-permute-done.first = bf16[2048,128]{1,0:T(8,128)(2,1)S(1)} collective-permute-done((bf16[2048,128]{1,0:T(8,128)(2,1)S(1)}, bf16[2048,128]{1,0:T(8,128)(2,1)S(1)}, u32[]{:S(2)}, u32[]{:S(2)}) %collective-permute-start) | collective-permute-done | bytes 524320 | tf_op jit(solution)/shard_map/ppermute | solution.py:457
  66.3 4.1 %collective-permute-start.1 = (bf16[2048,128]{1,0:T(8,128)(2,1)S(1)}, bf16[2048,128]{1,0:T(8,128)(2,1)S(1)}, u32[]{:S(2)}, u32[]{:S(2)}) collective-permute-start(bf16[2048,128]{1,0:T(8,128)(2,1)S(1)} %collective-permute-done.first), channel_id=1, source_target_pairs={{0,16},{16,0},{32,48},{48,32},{64,80},{80,64},{96,112},{112,96},{1... | collective-permute-start | bytes 1572872 | tf_op jit(solution)/shard_map/ppermute | solution.py:458
  70.4 0.8 copy-done.3
  71.9 0.8 copy-done.5
  72.7 1.0 copy-done.4
  73.8 1.0 copy-done.6
  74.8 6.4 %shard_map.106 = (f32[128,256]{1,0:T(8,128)S(1)}, f32[4,128,128]{2,1,0:T(8,128)S(1)}, bf16[4,128,128]{2,1,0:T(8,128)(2,1)S(1)}, bf16[4,128,128]{2,1,0:T(8,128)(2...) custom-call(bf16[16,528,128]{2,1,0:T(8,128)(2,1)S(1)} %all-to-all-done.1.xg, ...), custom_call_target="tpu_custom_call" | custom-call | tf_op jit(solution)/shard_map/pallas_call | solution.py:312
  81.2 1.9 %collective-permute-start.2 = (f32[128,256]{1,0:T(8,128)S(1)}, f32[128,256]{1,0:T(8,128)S(1)}, u32[]{:S(2)}, u32[]{:S(2)}) collective-permute-start(f32[128,256]{1,0:T(8,128)S(1)} %get-tuple-element.19), channel_id=1, source_target_pairs={{0,1},{1,0},{2,3},{3,2},{4,5},{5,4},{6,7},{7,6},{8,9},{9,8},{10,11... | collective-permute-start | bytes 393224 | tf_op jit(solution)/shard_map/ppermute | solution.py:469
  83.1 1.2 shard_map.107.mine
  84.3 3.5 %collective-permute-done.2.other = f32[128,256]{1,0:T(8,128)S(1)} collective-permute-done((f32[128,256]{1,0:T(8,128)S(1)}, f32[128,256]{1,0:T(8,128)S(1)}, u32[]{:S(2)}, u32[]{:S(2)}) %collective-permute-start.2) | collective-permute-done | bytes 131104 | tf_op jit(solution)/shard_map/ppermute | solution.py:469
  88.0 11.0 %collective-permute-start.3 = (bf16[144,256]{1,0:T(8,128)(2,1)S(1)}, bf16[144,256]{1,0:T(8,128)(2,1)S(1)}, u32[]{:S(2)}, u32[]{:S(2)}) collective-permute-start(bf16[144,256]{1,0:T(8,128)(2,1)S(1)} %shard_map.108), channel_id=1, source_target_pairs={{0,320},{16,384},{32,448},{48,0},{64,64},{80,128},{96,192},{112,25... | collective-permute-start | bytes 221192 | tf_op jit(solution)/shard_map/ppermute | solution.py:478
  99.0 1.9 %collective-permute-done.3.mine = bf16[144,256]{1,0:T(8,128)(2,1)S(1)} collective-permute-done((bf16[144,256]{1,0:T(8,128)(2,1)S(1)}, bf16[144,256]{1,0:T(8,128)(2,1)S(1)}, u32[]{:S(2)}, u32[]{:S(2)}) %collective-permute-start.3) | collective-permute-done | bytes 73760 | tf_op jit(solution)/shard_map/ppermute | solution.py:478
  101.0 1.9 %collective-permute-start.4 = (bf16[144,256]{1,0:T(8,128)(2,1)S(1)}, bf16[144,256]{1,0:T(8,128)(2,1)S(1)}, u32[]{:S(2)}, u32[]{:S(2)}) collective-permute-start(bf16[144,256]{1,0:T(8,128)(2,1)S(1)} %collective-permute-done.3.mine), channel_id=1, source_target_pairs={{0,16},{16,0},{32,48},{48,32},{64,80},{80,64},{96,112},{112,96},{1... | collective-permute-start | bytes 221192 | tf_op jit(solution)/shard_map/ppermute | solution.py:479
  102.9 1.2 collective-permute-done.4.other
  104.3 6.7 %collective-permute-start.5 = (f32[128,128]{1,0:T(8,128)S(1)}, f32[128,128]{1,0:T(8,128)S(1)}, u32[]{:S(2)}, u32[]{:S(2)}) collective-permute-start(f32[128,128]{1,0:T(8,128)S(1)} %get-tuple-element.21), channel_id=1, source_target_pairs={{0,32},{16,48},{32,0},{48,16},{64,96},{80,112},{96,64},{112,80},{1... | collective-permute-start | bytes 196616 | tf_op jit(solution)/shard_map/ppermute | solution.py:481
  111.0 2.1 %collective-permute-done.5.got = f32[128,128]{1,0:T(8,128)S(1)} collective-permute-done((f32[128,128]{1,0:T(8,128)S(1)}, f32[128,128]{1,0:T(8,128)S(1)}, u32[]{:S(2)}, u32[]{:S(2)}) %collective-permute-start.5) | collective-permute-done | bytes 65568 | tf_op jit(solution)/shard_map/ppermute | solution.py:481
  113.1 0.8 shard_map.110
  113.9 21.7 %all_to_all.15 = f32[32,1,128]{2,1,0:T(1,128)S(1)} all-to-all(f32[32,1,128]{2,1,0:T(1,128)S(1)} %broadcast_in_dim.5), channel_id=1, replica_groups=mesh['sp'=32,'tp'=16] {'sp'}, dimensions={0} | all-to-all | bytes 32768 | tf_op jit(solution)/shard_map/all_to_all | solution.py:484
  (26 shorter events, 2.3 us)
Async XLA Ops:
  2.3 19.5 %all-to-all-start = ((bf16[8,144,128]{2,1,0:T(8,128)(2,1)}), bf16[8,144,128]{2,1,0:T(8,128)(2,1)S(1)}, u32[]{:S(2)}, u32[]{:S(2)}) async-start(bf16[8,144,128]{2,1,0:T(8,128)(2,1)} %shard_map.104), calls=%async_computation | async-start | bytes 589824 | tf_op jit(solution)/shard_map/all_to_all | solution.py:462
  22.1 1.4 copy-start
  23.5 4.1 %copy-start.1 = (bf16[2048,128]{1,0:T(8,128)(2,1)S(1)}, bf16[2048,128]{1,0:T(8,128)(2,1)}, u32[]{:S(2)}) copy-start(bf16[2048,128]{1,0:T(8,128)(2,1)} %wk.1) | copy-start | bytes 1572868
  23.5 4.1 %copy-start.2 = (bf16[2048,128]{1,0:T(8,128)(2,1)S(1)}, bf16[2048,128]{1,0:T(8,128)(2,1)}, u32[]{:S(2)}) copy-start(bf16[2048,128]{1,0:T(8,128)(2,1)} %wv.1) | copy-start | bytes 1572868
  23.5 49.2 %copy-start.7 = (bf16[2,2048,16]{1,2,0:T(8,128)(2,1)S(1)}, bf16[2,2048,16]{1,2,0:T(8,128)(2,1)}, u32[]{:S(2)}) copy-start(bf16[2,2048,16]{1,2,0:T(8,128)(2,1)} %param.12) | copy-start | bytes 393220
  23.5 49.2 %all-to-all-start.1 = ((bf16[16,528,128]{2,1,0:T(8,128)(2,1)}), bf16[16,528,128]{2,1,0:T(8,128)(2,1)S(1)}, u32[]{:S(2)}, u32[]{:S(2)}) async-start(bf16[16,528,128]{2,1,0:T(8,128)(2,1)} %copy-done), calls=%async_computation.1 | async-start | bytes 4325376 | tf_op jit(solution)/shard_map/all_to_all | solution.py:465
  27.7 38.6 %collective-permute-start = (bf16[2048,128]{1,0:T(8,128)(2,1)S(1)}, bf16[2048,128]{1,0:T(8,128)(2,1)S(1)}, u32[]{:S(2)}, u32[]{:S(2)}) collective-permute-start(bf16[2048,128]{1,0:T(8,128)(2,1)S(1)} %broadcast_select_fusion), channel_id=1, source_target_pairs={{0,1},{1,0},{2,3},{3,2},{4,5},{5,4},{6,7},{7,6},{8,9},{9,8},{10,11... | collective-permute-start | bytes 1572872 | tf_op jit(solution)/shard_map/ppermute | solution.py:457
  66.3 5.6 %collective-permute-start.1 = (bf16[2048,128]{1,0:T(8,128)(2,1)S(1)}, bf16[2048,128]{1,0:T(8,128)(2,1)S(1)}, u32[]{:S(2)}, u32[]{:S(2)}) collective-permute-start(bf16[2048,128]{1,0:T(8,128)(2,1)S(1)} %collective-permute-done.first), channel_id=1, source_target_pairs={{0,16},{16,0},{32,48},{48,32},{64,80},{80,64},{96,112},{112,96},{1... | collective-permute-start | bytes 1572872 | tf_op jit(solution)/shard_map/ppermute | solution.py:458
  70.4 0.8 copy-start.3
  71.9 0.8 copy-start.5
  72.7 1.0 copy-start.4
  73.7 1.0 copy-start.6
  74.8 38.3 %copy-start.8 = (bf16[8,128]{1,0:T(8,128)(2,1)S(1)}, bf16[8,128]{1,0:T(8,128)(2,1)}, u32[]{:S(2)}) copy-start(bf16[8,128]{1,0:T(8,128)(2,1)} %query.1) | copy-start | bytes 6148
  74.8 60.9 %copy-start.9 = (f32[128]{0:T(128)S(1)}, f32[128]{0:T(128)}, u32[]{:S(2)}) copy-start(f32[128]{0:T(128)} %param.17) | copy-start | bytes 1540
  81.2 6.6 %collective-permute-start.2 = (f32[128,256]{1,0:T(8,128)S(1)}, f32[128,256]{1,0:T(8,128)S(1)}, u32[]{:S(2)}, u32[]{:S(2)}) collective-permute-start(f32[128,256]{1,0:T(8,128)S(1)} %get-tuple-element.19), channel_id=1, source_target_pairs={{0,1},{1,0},{2,3},{3,2},{4,5},{5,4},{6,7},{7,6},{8,9},{9,8},{10,11... | collective-permute-start | bytes 393224 | tf_op jit(solution)/shard_map/ppermute | solution.py:469
  88.0 13.0 %collective-permute-start.3 = (bf16[144,256]{1,0:T(8,128)(2,1)S(1)}, bf16[144,256]{1,0:T(8,128)(2,1)S(1)}, u32[]{:S(2)}, u32[]{:S(2)}) collective-permute-start(bf16[144,256]{1,0:T(8,128)(2,1)S(1)} %shard_map.108), channel_id=1, source_target_pairs={{0,320},{16,384},{32,448},{48,0},{64,64},{80,128},{96,192},{112,25... | collective-permute-start | bytes 221192 | tf_op jit(solution)/shard_map/ppermute | solution.py:478
  101.0 3.1 %collective-permute-start.4 = (bf16[144,256]{1,0:T(8,128)(2,1)S(1)}, bf16[144,256]{1,0:T(8,128)(2,1)S(1)}, u32[]{:S(2)}, u32[]{:S(2)}) collective-permute-start(bf16[144,256]{1,0:T(8,128)(2,1)S(1)} %collective-permute-done.3.mine), channel_id=1, source_target_pairs={{0,16},{16,0},{32,48},{48,32},{64,80},{80,64},{96,112},{112,96},{1... | collective-permute-start | bytes 221192 | tf_op jit(solution)/shard_map/ppermute | solution.py:479
  104.3 8.8 %collective-permute-start.5 = (f32[128,128]{1,0:T(8,128)S(1)}, f32[128,128]{1,0:T(8,128)S(1)}, u32[]{:S(2)}, u32[]{:S(2)}) collective-permute-start(f32[128,128]{1,0:T(8,128)S(1)} %get-tuple-element.21), channel_id=1, source_target_pairs={{0,32},{16,48},{32,0},{48,16},{64,96},{80,112},{96,64},{112,80},{1... | collective-permute-start | bytes 196616 | tf_op jit(solution)/shard_map/ppermute | solution.py:481

commit v5 on v3

--- a/solution.py
+++ b/solution.py
@@ -180,20 +180,25 @@
         step *= 2
 
 
-def partner_kernel(xg, first, second, wg, out, gates, *scratch):
-    *scratch, weights, sem = scratch
-    core = lax.axis_index("sp") % 2
-    copies = [
-        pltpu.make_async_copy(first, weights.at[core], sem.at[0]),
-        pltpu.make_async_copy(second, weights.at[1 - core], sem.at[1]),
-    ]
-    for copy in copies:
-        copy.start()
-    x = features(xg)
-    gates[...] = dot1(wg[...], x, NT)
-    for copy in copies:
-        copy.wait()
-    head_map(lax.axis_index("tp") ^ 1, x, xg, weights[0], weights[1], gates, out, *scratch)
+def gate_kernel(xg, wg, gates):
+    gates[...] = dot1(wg[...], features(xg), NT)
+
+
+def gate_sums(xg, gate_rows):
+    return pl.pallas_call(
+        gate_kernel,
+        in_specs=[VMEM] * 2,
+        out_specs=VMEM,
+        out_shape=jax.ShapeDtypeStruct((gate_rows.shape[0], xg.shape[1] - PAD), F32),
+        compiler_params=granted(8),
+    )(xg, gate_rows)
+
+
+def partner_kernel(xg, first, second, gates, out, *scratch):
+    turned = lax.axis_index("sp") % 2 == 1
+    w_key = jnp.where(turned, second[...], first[...])
+    w_value = jnp.where(turned, first[...], second[...])
+    head_map(lax.axis_index("tp") ^ 1, features(xg), xg, w_key, w_value, gates, out, *scratch)
 
 
 def own_kernel(xg, w_key, w_value, gates, out, *scratch):
@@ -281,14 +286,14 @@
     return jnp.concatenate([both[:, :DK], both[:, DK:] + later[:, DK:]], axis=1)
 
 
-def head_call(kernel, outs, more, used, specs, *operands):
+def head_call(kernel, *operands):
+    used = operands[0].shape[1] - PAD
     units = used // BLOCK
-    shape = jax.ShapeDtypeStruct((DK, DK + DV), F32)
     return pl.pallas_call(
         kernel,
-        in_specs=specs,
-        out_specs=[VMEM] * (1 + len(outs)),
-        out_shape=[shape, *outs],
+        in_specs=[VMEM] * len(operands),
+        out_specs=VMEM,
+        out_shape=jax.ShapeDtypeStruct((DK, DK + DV), F32),
         scratch_shapes=[
             pltpu.VMEM((used, DK + DV), F32),
             pltpu.VMEM((units, BLOCK, DK), F32),
@@ -299,7 +304,6 @@
             pltpu.VMEM((units, BLOCK, DK + DV), F32),
             pltpu.VMEM((units, BLOCK, DK + DV), BF16),
             pltpu.VMEM((units, DK, DK + DV), F32),
-            *more,
         ],
         compiler_params=granted(24),
     )(*operands)
@@ -431,19 +435,10 @@
     gathered = lax.all_to_all(parcel, "tp", 0, 0, tiled=True)
 
     gate_rows = w_gates.transpose(0, 2, 1).reshape(2 * tp, -1)
-    used = gathered.shape[1] - PAD
-    gate_shape = jax.ShapeDtypeStruct((gate_rows.shape[0], used), F32)
-    held = [pltpu.VMEM((2, *w_key.shape), BF16), pltpu.SemaphoreType.DMA((2,))]
-    theirs, gates = head_call(
-        partner_kernel,
-        [gate_shape],
-        held,
-        used,
-        [VMEM, HBM, HBM, VMEM],
-        *(gathered, first, second, gate_rows),
-    )
+    gates = gate_sums(gathered, gate_rows)
+    theirs = head_call(partner_kernel, gathered, first, second, gates)
     other = lax.ppermute(theirs, "tp", pair)
-    (mine,) = head_call(own_kernel, [], [], used, [VMEM] * 4, gathered, w_key, w_value, gates)
+    mine = head_call(own_kernel, gathered, w_key, w_value, gates)
     whole = pair_composed(mine, other)
 
     ways = [

time: 136 us -> 134 us (0.985)
  local copies, waits for them, and re-layouts: 5.04 us -> 1.38 us
    unnamed x20 -> x12, local copies, waits for them, and re-layouts: 5.03 us -> 1.37 us
    pallas_call x2 -> x3, Pallas kernels: 9.39 us -> 10.5 us  [the longest x2 9.78 us: head_call(): pl.pallas_call(kernel, in_specs=[VMEM] * len(operands), out_specs=VMEM, o...]
  transfers between devices with their start and end apart: 8 -> 8, of which waited for: 7 -> 7; matrix products, arithmetic and copies ran while one was open for 0% -> 0% of each run, Pallas kernels for 3% -> 4%
where the time goes in v5:
time: 134 us; the launch traced here: 133 us
  waiting for transfers between devices  50.3 us (38%)
  starting transfers between devices  43.1 us (32%)
  blocking collectives  21.7 us (16%)
  Pallas kernels  13.6 us (10%)
  between operations  2.11 us (2%)
  local copies, waits for them, and re-layouts  1.38 us (1%)
    ppermute x1, waiting for transfers between devices, shards(): first = lax.ppermute(picked, 'tp', pair)  35.5 us
    all_to_all x1, blocking collectives, shards(): lax.all_to_all(jnp.broadcast_to(partial[None], (sp, 1, DV)), 'sp', 0, 0,...  21.7 us
    ppermute x1, starting transfers between devices, shards(): moved = lax.ppermute(whole, 'sp', ways)  11 us
    all_to_all x1, starting transfers between devices, shards(): lax.all_to_all(sent, 'sp', 0, 0, axis_index_groups=groups, tiled=True)  10.2 us
    pallas_call x2, Pallas kernels, head_call(): pl.pallas_call(kernel, in_specs=[VMEM] * len(operands), out_specs=VMEM, o...  9.78 us
    all_to_all x1, waiting for transfers between devices, shards(): lax.all_to_all(sent, 'sp', 0, 0, axis_index_groups=groups, tiled=True)  8.06 us
    ppermute x1, starting transfers between devices, shards(): got = lax.ppermute(give, 'sp', [(i, i ^ 2) for i in range(sp)])  6.67 us
    all_to_all x1, starting transfers between devices, shards(): gathered = lax.all_to_all(parcel, 'tp', 0, 0, tiled=True)  4.09 us
  transfers between devices with their start and end apart: 8, of which 7 were waited for; matrix products, arithmetic and copies ran while one was open for 0% of the time, Pallas kernels for 4%

profile of v5, /device:TPU:1, one launch (start us, length us, event | category | flops | bytes accessed | tf_op | source)
XLA Modules:
  0.0 133.0 jit_solution(1035317912026870122)
XLA Ops:
  0.6 1.7 %shard_map.104 = bf16[8,144,128]{2,1,0:T(8,128)(2,1)} custom-call(bf16[8,128,128]{2,1,0:T(8,128)(2,1)} %x.1, f32[8,128]{1,0:T(8,128)} %bitcast.9), custom_call_target="tpu_custom_call" | custom-call | tf_op jit(solution)/shard_map/pallas_call | solution.py:114
  2.3 10.2 %all-to-all-start = ((bf16[8,144,128]{2,1,0:T(8,128)(2,1)}), bf16[8,144,128]{2,1,0:T(8,128)(2,1)S(1)}, u32[]{:S(2)}, u32[]{:S(2)}) async-start(bf16[8,144,128]{2,1,0:T(8,128)(2,1)} %shard_map.104), calls=%async_computation | async-start | bytes 589824 | tf_op jit(solution)/shard_map/all_to_all | solution.py:432
  13.8 8.1 %all-to-all-done.here = bf16[8,144,128]{2,1,0:T(8,128)(2,1)S(1)} async-done(((bf16[8,144,128]{2,1,0:T(8,128)(2,1)}), bf16[8,144,128]{2,1,0:T(8,128)(2,1)S(1)}, u32[]{:S(2)}, u32[]{:S(2)}) %all-to-all-start) | async-done | bytes 294944 | tf_op jit(solution)/shard_map/all_to_all | solution.py:432
  21.9 0.3 shard_map.105
  22.2 1.3 %copy-done = bf16[16,528,128]{2,1,0:T(8,128)(2,1)} copy-done((bf16[16,528,128]{2,1,0:T(8,128)(2,1)}, bf16[16,528,128]{2,1,0:T(8,128)(2,1)S(1)}, u32[]{:S(2)}) %copy-start) | copy-done | bytes 2162712
  23.5 4.1 %all-to-all-start.1 = ((bf16[16,528,128]{2,1,0:T(8,128)(2,1)}), bf16[16,528,128]{2,1,0:T(8,128)(2,1)S(1)}, u32[]{:S(2)}, u32[]{:S(2)}) async-start(bf16[16,528,128]{2,1,0:T(8,128)(2,1)} %copy-done), calls=%async_computation.1 | async-start | bytes 4325376 | tf_op jit(solution)/shard_map/all_to_all | solution.py:435
  27.7 3.3 %collective-permute-start = (bf16[2048,128]{1,0:T(8,128)(2,1)S(1)}, bf16[2048,128]{1,0:T(8,128)(2,1)}, u32[]{:S(2)}, u32[]{:S(2)}) collective-permute-start(bf16[2048,128]{1,0:T(8,128)(2,1)S(1)} %broadcast_select_fusion), channel_id=1, source_target_pairs={{0,1},{1,0},{2,3},{3,2},{4,5},{5,4},{6,7},{7,6},{8,9},{9,8},{10,11... | collective-permute-start | bytes 1572872 | tf_op jit(solution)/shard_map/ppermute | solution.py:427
  31.0 35.5 %collective-permute-done.first = bf16[2048,128]{1,0:T(8,128)(2,1)} collective-permute-done((bf16[2048,128]{1,0:T(8,128)(2,1)S(1)}, bf16[2048,128]{1,0:T(8,128)(2,1)}, u32[]{:S(2)}, u32[]{:S(2)}) %collective-permute-start) | collective-permute-done | bytes 524320 | tf_op jit(solution)/shard_map/ppermute | solution.py:427
  66.4 4.1 %collective-permute-start.1 = (bf16[2048,128]{1,0:T(8,128)(2,1)}, bf16[2048,128]{1,0:T(8,128)(2,1)}, u32[]{:S(2)}, u32[]{:S(2)}) collective-permute-start(bf16[2048,128]{1,0:T(8,128)(2,1)} %collective-permute-done.first), channel_id=1, source_target_pairs={{0,16},{16,0},{32,48},{48,32},{64,80},{80,64},{96,112},{112,96},{1... | collective-permute-start | bytes 1572872 | tf_op jit(solution)/shard_map/ppermute | solution.py:428
  70.5 0.7 shard_map.106.gates
  71.2 1.1 collective-permute-done.1.second
  72.4 5.5 %shard_map.108 = f32[128,256]{1,0:T(8,128)S(1)} custom-call(bf16[16,528,128]{2,1,0:T(8,128)(2,1)S(1)} %all-to-all-done.1.xg, bf16[2048,128]{1,0:T(8,128)(2,1)} %collective-permute-done.first, bf16[2048,128]{1,0:T(8,128)(2,1)} %collective-permute-done.1.second, f32[32,512]{1,0:T(8,128)S(1)} %shard_map.106.gates), custom_call_target="tpu_custom_call" | custom-call | tf_op jit(solution)/shard_map/pallas_call | solution.py:292
  77.9 1.9 %collective-permute-start.2 = (f32[128,256]{1,0:T(8,128)S(1)}, f32[128,256]{1,0:T(8,128)S(1)}, u32[]{:S(2)}, u32[]{:S(2)}) collective-permute-start(f32[128,256]{1,0:T(8,128)S(1)} %shard_map.108), channel_id=1, source_target_pairs={{0,1},{1,0},{2,3},{3,2},{4,5},{5,4},{6,7},{7,6},{8,9},{9,8},{10,11... | collective-permute-start | bytes 393224 | tf_op jit(solution)/shard_map/ppermute | solution.py:440
  79.8 4.3 %shard_map.107.mine = f32[128,256]{1,0:T(8,128)S(1)} custom-call(bf16[16,528,128]{2,1,0:T(8,128)(2,1)S(1)} %all-to-all-done.1.xg, bf16[2048,128]{1,0:T(8,128)(2,1)S(1)} %copy-done.1, bf16[2048,128]{1,0:T(8,128)(2,1)S(1)} %copy-done.2, f32[32,512]{1,0:T(8,128)S(1)} %shard_map.106.gates), custom_call_target="tpu_custom_call" | custom-call | tf_op jit(solution)/shard_map/pallas_call | solution.py:292
  84.1 0.3 collective-permute-done.2.other
  84.7 11.0 %collective-permute-start.3 = (bf16[144,256]{1,0:T(8,128)(2,1)S(1)}, bf16[144,256]{1,0:T(8,128)(2,1)S(1)}, u32[]{:S(2)}, u32[]{:S(2)}) collective-permute-start(bf16[144,256]{1,0:T(8,128)(2,1)S(1)} %shard_map.109), channel_id=1, source_target_pairs={{0,320},{16,384},{32,448},{48,0},{64,64},{80,128},{96,192},{112,25... | collective-permute-start | bytes 221192 | tf_op jit(solution)/shard_map/ppermute | solution.py:449
  95.7 1.9 %collective-permute-done.3.mine = bf16[144,256]{1,0:T(8,128)(2,1)S(1)} collective-permute-done((bf16[144,256]{1,0:T(8,128)(2,1)S(1)}, bf16[144,256]{1,0:T(8,128)(2,1)S(1)}, u32[]{:S(2)}, u32[]{:S(2)}) %collective-permute-start.3) | collective-permute-done | bytes 73760 | tf_op jit(solution)/shard_map/ppermute | solution.py:449
  97.6 1.9 %collective-permute-start.4 = (bf16[144,256]{1,0:T(8,128)(2,1)S(1)}, bf16[144,256]{1,0:T(8,128)(2,1)S(1)}, u32[]{:S(2)}, u32[]{:S(2)}) collective-permute-start(bf16[144,256]{1,0:T(8,128)(2,1)S(1)} %collective-permute-done.3.mine), channel_id=1, source_target_pairs={{0,16},{16,0},{32,48},{48,32},{64,80},{80,64},{96,112},{112,96},{1... | collective-permute-start | bytes 221192 | tf_op jit(solution)/shard_map/ppermute | solution.py:450
  99.6 1.2 collective-permute-done.4.other
  101.0 6.7 %collective-permute-start.5 = (f32[128,128]{1,0:T(8,128)S(1)}, f32[128,128]{1,0:T(8,128)S(1)}, u32[]{:S(2)}, u32[]{:S(2)}) collective-permute-start(f32[128,128]{1,0:T(8,128)S(1)} %get-tuple-element.7), channel_id=1, source_target_pairs={{0,32},{16,48},{32,0},{48,16},{64,96},{80,112},{96,64},{112,80},{1... | collective-permute-start | bytes 196616 | tf_op jit(solution)/shard_map/ppermute | solution.py:452
  107.7 2.1 %collective-permute-done.5.got = f32[128,128]{1,0:T(8,128)S(1)} collective-permute-done((f32[128,128]{1,0:T(8,128)S(1)}, f32[128,128]{1,0:T(8,128)S(1)}, u32[]{:S(2)}, u32[]{:S(2)}) %collective-permute-start.5) | collective-permute-done | bytes 65568 | tf_op jit(solution)/shard_map/ppermute | solution.py:452
  109.8 0.8 shard_map.111
  110.6 21.7 %all_to_all.15 = f32[32,1,128]{2,1,0:T(1,128)S(1)} all-to-all(f32[32,1,128]{2,1,0:T(1,128)S(1)} %broadcast_in_dim.5), channel_id=1, replica_groups=mesh['sp'=32,'tp'=16] {'sp'}, dimensions={0} | all-to-all | bytes 32768 | tf_op jit(solution)/shard_map/all_to_all | solution.py:455
  132.4 0.7 multiply_convert_fusion
  (19 shorter events, 0.7 us)
Async XLA Ops:
  2.3 19.5 %all-to-all-start = ((bf16[8,144,128]{2,1,0:T(8,128)(2,1)}), bf16[8,144,128]{2,1,0:T(8,128)(2,1)S(1)}, u32[]{:S(2)}, u32[]{:S(2)}) async-start(bf16[8,144,128]{2,1,0:T(8,128)(2,1)} %shard_map.104), calls=%async_computation | async-start | bytes 589824 | tf_op jit(solution)/shard_map/all_to_all | solution.py:432
  22.2 1.4 %copy-start = (bf16[16,528,128]{2,1,0:T(8,128)(2,1)}, bf16[16,528,128]{2,1,0:T(8,128)(2,1)S(1)}, u32[]{:S(2)}) copy-start(bf16[16,528,128]{2,1,0:T(8,128)(2,1)S(1)} %shard_map.105) | copy-start | bytes 6488068
  23.5 4.1 %copy-start.1 = (bf16[2048,128]{1,0:T(8,128)(2,1)S(1)}, bf16[2048,128]{1,0:T(8,128)(2,1)}, u32[]{:S(2)}) copy-start(bf16[2048,128]{1,0:T(8,128)(2,1)} %w_key.1) | copy-start | bytes 1572868
  23.5 4.1 %copy-start.2 = (bf16[2048,128]{1,0:T(8,128)(2,1)S(1)}, bf16[2048,128]{1,0:T(8,128)(2,1)}, u32[]{:S(2)}) copy-start(bf16[2048,128]{1,0:T(8,128)(2,1)} %w_value.1) | copy-start | bytes 1572868
  23.5 47.0 %copy-start.3 = (bf16[2,2048,16]{1,2,0:T(8,128)(2,1)S(1)}, bf16[2,2048,16]{1,2,0:T(8,128)(2,1)}, u32[]{:S(2)}) copy-start(bf16[2,2048,16]{1,2,0:T(8,128)(2,1)} %param.12) | copy-start | bytes 393220
  23.5 47.0 %all-to-all-start.1 = ((bf16[16,528,128]{2,1,0:T(8,128)(2,1)}), bf16[16,528,128]{2,1,0:T(8,128)(2,1)S(1)}, u32[]{:S(2)}, u32[]{:S(2)}) async-start(bf16[16,528,128]{2,1,0:T(8,128)(2,1)} %copy-done), calls=%async_computation.1 | async-start | bytes 4325376 | tf_op jit(solution)/shard_map/all_to_all | solution.py:435
  27.7 38.7 %collective-permute-start = (bf16[2048,128]{1,0:T(8,128)(2,1)S(1)}, bf16[2048,128]{1,0:T(8,128)(2,1)}, u32[]{:S(2)}, u32[]{:S(2)}) collective-permute-start(bf16[2048,128]{1,0:T(8,128)(2,1)S(1)} %broadcast_select_fusion), channel_id=1, source_target_pairs={{0,1},{1,0},{2,3},{3,2},{4,5},{5,4},{6,7},{7,6},{8,9},{9,8},{10,11... | collective-permute-start | bytes 1572872 | tf_op jit(solution)/shard_map/ppermute | solution.py:427
  66.4 5.9 %collective-permute-start.1 = (bf16[2048,128]{1,0:T(8,128)(2,1)}, bf16[2048,128]{1,0:T(8,128)(2,1)}, u32[]{:S(2)}, u32[]{:S(2)}) collective-permute-start(bf16[2048,128]{1,0:T(8,128)(2,1)} %collective-permute-done.first), channel_id=1, source_target_pairs={{0,16},{16,0},{32,48},{48,32},{64,80},{80,64},{96,112},{112,96},{1... | collective-permute-start | bytes 1572872 | tf_op jit(solution)/shard_map/ppermute | solution.py:428
  77.9 31.9 %copy-start.4 = (bf16[8,128]{1,0:T(8,128)(2,1)S(1)}, bf16[8,128]{1,0:T(8,128)(2,1)}, u32[]{:S(2)}) copy-start(bf16[8,128]{1,0:T(8,128)(2,1)} %query.1) | copy-start | bytes 6148
  77.9 54.5 %copy-start.5 = (f32[128]{0:T(128)S(1)}, f32[128]{0:T(128)}, u32[]{:S(2)}) copy-start(f32[128]{0:T(128)} %param.17) | copy-start | bytes 1540
  77.9 6.6 %collective-permute-start.2 = (f32[128,256]{1,0:T(8,128)S(1)}, f32[128,256]{1,0:T(8,128)S(1)}, u32[]{:S(2)}, u32[]{:S(2)}) collective-permute-start(f32[128,256]{1,0:T(8,128)S(1)} %shard_map.108), channel_id=1, source_target_pairs={{0,1},{1,0},{2,3},{3,2},{4,5},{5,4},{6,7},{7,6},{8,9},{9,8},{10,11... | collective-permute-start | bytes 393224 | tf_op jit(solution)/shard_map/ppermute | solution.py:440
  84.7 13.0 %collective-permute-start.3 = (bf16[144,256]{1,0:T(8,128)(2,1)S(1)}, bf16[144,256]{1,0:T(8,128)(2,1)S(1)}, u32[]{:S(2)}, u32[]{:S(2)}) collective-permute-start(bf16[144,256]{1,0:T(8,128)(2,1)S(1)} %shard_map.109), channel_id=1, source_target_pairs={{0,320},{16,384},{32,448},{48,0},{64,64},{80,128},{96,192},{112,25... | collective-permute-start | bytes 221192 | tf_op jit(solution)/shard_map/ppermute | solution.py:449
  97.6 3.1 %collective-permute-start.4 = (bf16[144,256]{1,0:T(8,128)(2,1)S(1)}, bf16[144,256]{1,0:T(8,128)(2,1)S(1)}, u32[]{:S(2)}, u32[]{:S(2)}) collective-permute-start(bf16[144,256]{1,0:T(8,128)(2,1)S(1)} %collective-permute-done.3.mine), channel_id=1, source_target_pairs={{0,16},{16,0},{32,48},{48,32},{64,80},{80,64},{96,112},{112,96},{1... | collective-permute-start | bytes 221192 | tf_op jit(solution)/shard_map/ppermute | solution.py:450
  101.0 8.8 %collective-permute-start.5 = (f32[128,128]{1,0:T(8,128)S(1)}, f32[128,128]{1,0:T(8,128)S(1)}, u32[]{:S(2)}, u32[]{:S(2)}) collective-permute-start(f32[128,128]{1,0:T(8,128)S(1)} %get-tuple-element.7), channel_id=1, source_target_pairs={{0,32},{16,48},{32,0},{48,16},{64,96},{80,112},{96,64},{112,80},{1... | collective-permute-start | bytes 196616 | tf_op jit(solution)/shard_map/ppermute | solution.py:452

commit v6 on v5

--- a/solution.py
+++ b/solution.py
@@ -90,33 +90,44 @@
     return high, mid, (rest - mid).astype(BF16).astype(F32)
 
 
-def pack_kernel(x, extra, out, held, sem):
+def pack_kernel(x, extra, out, staged, held, arrive, leave):
     prompts, seg, width = x.shape
     first = lax.axis_index("sp") // prompts * 2 + SHIFT
     which = lambda i: lax.rem(first + i, prompts)
-    copies = [
-        pltpu.make_async_copy(x.at[which(i)], out.at[i, pl.ds(0, seg)], sem.at[i])
+    extras = pltpu.make_async_copy(extra, held, arrive.at[prompts])
+    extras.start()
+    coming = [
+        pltpu.make_async_copy(x.at[which(i)], staged.at[i, pl.ds(0, seg)], arrive.at[i])
         for i in range(prompts)
     ]
-    copies.append(pltpu.make_async_copy(extra, held, sem.at[prompts]))
-    for copy in reversed(copies):
+    for copy in coming:
         copy.start()
-    copies[-1].wait()
+    extras.wait()
     for i in range(prompts):
         rows = list(three_pieces(held[pl.ds(which(i), 1), :])) + [jnp.zeros((PAD - 3, width), F32)]
-        out[i, seg:, :] = jnp.concatenate(rows, axis=0).astype(BF16)
-    for copy in copies[:-1]:
-        copy.wait()
+        staged[i, seg:, :] = jnp.concatenate(rows, axis=0).astype(BF16)
+    going = [pltpu.make_async_copy(staged.at[i], out.at[i], leave.at[i]) for i in range(prompts)]
+    for came, go in zip(coming, going):
+        came.wait()
+        go.start()
+    for go in going:
+        go.wait()
 
 
 def packed(layer_input, extra):
     prompts, seg, width = layer_input.shape
+    shape = (prompts, seg + PAD, width)
     return pl.pallas_call(
         pack_kernel,
         in_specs=[HBM, HBM],
-        out_specs=VMEM,
-        out_shape=jax.ShapeDtypeStruct((prompts, seg + PAD, width), BF16),
-        scratch_shapes=[pltpu.VMEM(extra.shape, F32), pltpu.SemaphoreType.DMA((prompts + 1,))],
+        out_specs=HBM,
+        out_shape=jax.ShapeDtypeStruct(shape, BF16),
+        scratch_shapes=[
+            pltpu.VMEM(shape, BF16),
+            pltpu.VMEM(extra.shape, F32),
+            pltpu.SemaphoreType.DMA((prompts + 1,)),
+            pltpu.SemaphoreType.DMA((prompts,)),
+        ],
         compiler_params=granted(60),
     )(layer_input, extra)
 

time: 134 us -> 134 us (level)
  no operation moved by 1% of the time
where the time goes in v6:
time: 134 us; the launch traced here: 133 us
  waiting for transfers between devices  50.3 us (38%)
  starting transfers between devices  43.1 us (32%)
  blocking collectives  21.7 us (16%)
  Pallas kernels  13.6 us (10%)
  between operations  2.11 us (2%)
  local copies, waits for them, and re-layouts  1.38 us (1%)
    ppermute x1, waiting for transfers between devices, shards(): first = lax.ppermute(picked, 'tp', pair)  35.5 us
    all_to_all x1, blocking collectives, shards(): lax.all_to_all(jnp.broadcast_to(partial[None], (sp, 1, DV)), 'sp', 0, 0,...  21.7 us
    ppermute x1, starting transfers between devices, shards(): moved = lax.ppermute(whole, 'sp', ways)  11 us
    all_to_all x1, starting transfers between devices, shards(): lax.all_to_all(sent, 'sp', 0, 0, axis_index_groups=groups, tiled=True)  10.2 us
    pallas_call x2, Pallas kernels, head_call(): pl.pallas_call(kernel, in_specs=[VMEM] * len(operands), out_specs=VMEM, o...  9.78 us
    all_to_all x1, waiting for transfers between devices, shards(): lax.all_to_all(sent, 'sp', 0, 0, axis_index_groups=groups, tiled=True)  8.06 us
    ppermute x1, starting transfers between devices, shards(): got = lax.ppermute(give, 'sp', [(i, i ^ 2) for i in range(sp)])  6.67 us
    all_to_all x1, starting transfers between devices, shards(): gathered = lax.all_to_all(parcel, 'tp', 0, 0, tiled=True)  4.09 us
  transfers between devices with their start and end apart: 8, of which 7 were waited for; matrix products, arithmetic and copies ran while one was open for 0% of the time, Pallas kernels for 4%

profile of v6, /device:TPU:1, one launch (start us, length us, event | category | flops | bytes accessed | tf_op | source)
XLA Modules:
  0.0 133.0 jit_solution(3867615259823618979)
XLA Ops:
  0.6 1.7 %shard_map.104 = bf16[8,144,128]{2,1,0:T(8,128)(2,1)} custom-call(bf16[8,128,128]{2,1,0:T(8,128)(2,1)} %x.1, f32[8,128]{1,0:T(8,128)} %bitcast.9), custom_call_target="tpu_custom_call" | custom-call | tf_op jit(solution)/shard_map/pallas_call | solution.py:120
  2.3 10.2 %all-to-all-start = ((bf16[8,144,128]{2,1,0:T(8,128)(2,1)}), bf16[8,144,128]{2,1,0:T(8,128)(2,1)S(1)}, u32[]{:S(2)}, u32[]{:S(2)}) async-start(bf16[8,144,128]{2,1,0:T(8,128)(2,1)} %shard_map.104), calls=%async_computation | async-start | bytes 589824 | tf_op jit(solution)/shard_map/all_to_all | solution.py:443
  13.8 8.1 %all-to-all-done.here = bf16[8,144,128]{2,1,0:T(8,128)(2,1)S(1)} async-done(((bf16[8,144,128]{2,1,0:T(8,128)(2,1)}), bf16[8,144,128]{2,1,0:T(8,128)(2,1)S(1)}, u32[]{:S(2)}, u32[]{:S(2)}) %all-to-all-start) | async-done | bytes 294944 | tf_op jit(solution)/shard_map/all_to_all | solution.py:443
  21.8 0.3 shard_map.105
  22.1 1.3 %copy-done = bf16[16,528,128]{2,1,0:T(8,128)(2,1)} copy-done((bf16[16,528,128]{2,1,0:T(8,128)(2,1)}, bf16[16,528,128]{2,1,0:T(8,128)(2,1)S(1)}, u32[]{:S(2)}) %copy-start) | copy-done | bytes 2162712
  23.5 4.1 %all-to-all-start.1 = ((bf16[16,528,128]{2,1,0:T(8,128)(2,1)}), bf16[16,528,128]{2,1,0:T(8,128)(2,1)S(1)}, u32[]{:S(2)}, u32[]{:S(2)}) async-start(bf16[16,528,128]{2,1,0:T(8,128)(2,1)} %copy-done), calls=%async_computation.1 | async-start | bytes 4325376 | tf_op jit(solution)/shard_map/all_to_all | solution.py:446
  27.7 3.3 %collective-permute-start = (bf16[2048,128]{1,0:T(8,128)(2,1)S(1)}, bf16[2048,128]{1,0:T(8,128)(2,1)}, u32[]{:S(2)}, u32[]{:S(2)}) collective-permute-start(bf16[2048,128]{1,0:T(8,128)(2,1)S(1)} %broadcast_select_fusion), channel_id=1, source_target_pairs={{0,1},{1,0},{2,3},{3,2},{4,5},{5,4},{6,7},{7,6},{8,9},{9,8},{10,11... | collective-permute-start | bytes 1572872 | tf_op jit(solution)/shard_map/ppermute | solution.py:438
  30.9 35.5 %collective-permute-done.first = bf16[2048,128]{1,0:T(8,128)(2,1)} collective-permute-done((bf16[2048,128]{1,0:T(8,128)(2,1)S(1)}, bf16[2048,128]{1,0:T(8,128)(2,1)}, u32[]{:S(2)}, u32[]{:S(2)}) %collective-permute-start) | collective-permute-done | bytes 524320 | tf_op jit(solution)/shard_map/ppermute | solution.py:438
  66.4 4.1 %collective-permute-start.1 = (bf16[2048,128]{1,0:T(8,128)(2,1)}, bf16[2048,128]{1,0:T(8,128)(2,1)}, u32[]{:S(2)}, u32[]{:S(2)}) collective-permute-start(bf16[2048,128]{1,0:T(8,128)(2,1)} %collective-permute-done.first), channel_id=1, source_target_pairs={{0,16},{16,0},{32,48},{48,32},{64,80},{80,64},{96,112},{112,96},{1... | collective-permute-start | bytes 1572872 | tf_op jit(solution)/shard_map/ppermute | solution.py:439
  70.5 0.7 shard_map.106.gates
  71.2 1.1 collective-permute-done.1.second
  72.3 5.5 %shard_map.108 = f32[128,256]{1,0:T(8,128)S(1)} custom-call(bf16[16,528,128]{2,1,0:T(8,128)(2,1)S(1)} %all-to-all-done.1.xg, bf16[2048,128]{1,0:T(8,128)(2,1)} %collective-permute-done.first, bf16[2048,128]{1,0:T(8,128)(2,1)} %collective-permute-done.1.second, f32[32,512]{1,0:T(8,128)S(1)} %shard_map.106.gates), custom_call_target="tpu_custom_call" | custom-call | tf_op jit(solution)/shard_map/pallas_call | solution.py:303
  77.8 1.9 %collective-permute-start.2 = (f32[128,256]{1,0:T(8,128)S(1)}, f32[128,256]{1,0:T(8,128)S(1)}, u32[]{:S(2)}, u32[]{:S(2)}) collective-permute-start(f32[128,256]{1,0:T(8,128)S(1)} %shard_map.108), channel_id=1, source_target_pairs={{0,1},{1,0},{2,3},{3,2},{4,5},{5,4},{6,7},{7,6},{8,9},{9,8},{10,11... | collective-permute-start | bytes 393224 | tf_op jit(solution)/shard_map/ppermute | solution.py:451
  79.8 4.3 %shard_map.107.mine = f32[128,256]{1,0:T(8,128)S(1)} custom-call(bf16[16,528,128]{2,1,0:T(8,128)(2,1)S(1)} %all-to-all-done.1.xg, bf16[2048,128]{1,0:T(8,128)(2,1)S(1)} %copy-done.1, bf16[2048,128]{1,0:T(8,128)(2,1)S(1)} %copy-done.2, f32[32,512]{1,0:T(8,128)S(1)} %shard_map.106.gates), custom_call_target="tpu_custom_call" | custom-call | tf_op jit(solution)/shard_map/pallas_call | solution.py:303
  84.1 0.3 collective-permute-done.2.other
  84.6 11.0 %collective-permute-start.3 = (bf16[144,256]{1,0:T(8,128)(2,1)S(1)}, bf16[144,256]{1,0:T(8,128)(2,1)S(1)}, u32[]{:S(2)}, u32[]{:S(2)}) collective-permute-start(bf16[144,256]{1,0:T(8,128)(2,1)S(1)} %shard_map.109), channel_id=1, source_target_pairs={{0,320},{16,384},{32,448},{48,0},{64,64},{80,128},{96,192},{112,25... | collective-permute-start | bytes 221192 | tf_op jit(solution)/shard_map/ppermute | solution.py:460
  95.7 1.9 %collective-permute-done.3.mine = bf16[144,256]{1,0:T(8,128)(2,1)S(1)} collective-permute-done((bf16[144,256]{1,0:T(8,128)(2,1)S(1)}, bf16[144,256]{1,0:T(8,128)(2,1)S(1)}, u32[]{:S(2)}, u32[]{:S(2)}) %collective-permute-start.3) | collective-permute-done | bytes 73760 | tf_op jit(solution)/shard_map/ppermute | solution.py:460
  97.6 1.9 %collective-permute-start.4 = (bf16[144,256]{1,0:T(8,128)(2,1)S(1)}, bf16[144,256]{1,0:T(8,128)(2,1)S(1)}, u32[]{:S(2)}, u32[]{:S(2)}) collective-permute-start(bf16[144,256]{1,0:T(8,128)(2,1)S(1)} %collective-permute-done.3.mine), channel_id=1, source_target_pairs={{0,16},{16,0},{32,48},{48,32},{64,80},{80,64},{96,112},{112,96},{1... | collective-permute-start | bytes 221192 | tf_op jit(solution)/shard_map/ppermute | solution.py:461
  99.5 1.2 collective-permute-done.4.other
  101.0 6.7 %collective-permute-start.5 = (f32[128,128]{1,0:T(8,128)S(1)}, f32[128,128]{1,0:T(8,128)S(1)}, u32[]{:S(2)}, u32[]{:S(2)}) collective-permute-start(f32[128,128]{1,0:T(8,128)S(1)} %get-tuple-element.7), channel_id=1, source_target_pairs={{0,32},{16,48},{32,0},{48,16},{64,96},{80,112},{96,64},{112,80},{1... | collective-permute-start | bytes 196616 | tf_op jit(solution)/shard_map/ppermute | solution.py:463
  107.6 2.1 %collective-permute-done.5.got = f32[128,128]{1,0:T(8,128)S(1)} collective-permute-done((f32[128,128]{1,0:T(8,128)S(1)}, f32[128,128]{1,0:T(8,128)S(1)}, u32[]{:S(2)}, u32[]{:S(2)}) %collective-permute-start.5) | collective-permute-done | bytes 65568 | tf_op jit(solution)/shard_map/ppermute | solution.py:463
  109.7 0.8 shard_map.111
  110.5 21.7 %all_to_all.15 = f32[32,1,128]{2,1,0:T(1,128)S(1)} all-to-all(f32[32,1,128]{2,1,0:T(1,128)S(1)} %broadcast_in_dim.5), channel_id=1, replica_groups=mesh['sp'=32,'tp'=16] {'sp'}, dimensions={0} | all-to-all | bytes 32768 | tf_op jit(solution)/shard_map/all_to_all | solution.py:466
  132.3 0.7 multiply_convert_fusion
  (19 shorter events, 0.7 us)
Async XLA Ops:
  2.3 19.5 %all-to-all-start = ((bf16[8,144,128]{2,1,0:T(8,128)(2,1)}), bf16[8,144,128]{2,1,0:T(8,128)(2,1)S(1)}, u32[]{:S(2)}, u32[]{:S(2)}) async-start(bf16[8,144,128]{2,1,0:T(8,128)(2,1)} %shard_map.104), calls=%async_computation | async-start | bytes 589824 | tf_op jit(solution)/shard_map/all_to_all | solution.py:443
  22.1 1.4 %copy-start = (bf16[16,528,128]{2,1,0:T(8,128)(2,1)}, bf16[16,528,128]{2,1,0:T(8,128)(2,1)S(1)}, u32[]{:S(2)}) copy-start(bf16[16,528,128]{2,1,0:T(8,128)(2,1)S(1)} %shard_map.105) | copy-start | bytes 6488068
  23.5 4.1 %copy-start.1 = (bf16[2048,128]{1,0:T(8,128)(2,1)S(1)}, bf16[2048,128]{1,0:T(8,128)(2,1)}, u32[]{:S(2)}) copy-start(bf16[2048,128]{1,0:T(8,128)(2,1)} %w_key.1) | copy-start | bytes 1572868
  23.5 4.1 %copy-start.2 = (bf16[2048,128]{1,0:T(8,128)(2,1)S(1)}, bf16[2048,128]{1,0:T(8,128)(2,1)}, u32[]{:S(2)}) copy-start(bf16[2048,128]{1,0:T(8,128)(2,1)} %w_value.1) | copy-start | bytes 1572868
  23.5 47.0 %copy-start.3 = (bf16[2,2048,16]{1,2,0:T(8,128)(2,1)S(1)}, bf16[2,2048,16]{1,2,0:T(8,128)(2,1)}, u32[]{:S(2)}) copy-start(bf16[2,2048,16]{1,2,0:T(8,128)(2,1)} %param.12) | copy-start | bytes 393220
  23.5 47.0 %all-to-all-start.1 = ((bf16[16,528,128]{2,1,0:T(8,128)(2,1)}), bf16[16,528,128]{2,1,0:T(8,128)(2,1)S(1)}, u32[]{:S(2)}, u32[]{:S(2)}) async-start(bf16[16,528,128]{2,1,0:T(8,128)(2,1)} %copy-done), calls=%async_computation.1 | async-start | bytes 4325376 | tf_op jit(solution)/shard_map/all_to_all | solution.py:446
  27.7 38.7 %collective-permute-start = (bf16[2048,128]{1,0:T(8,128)(2,1)S(1)}, bf16[2048,128]{1,0:T(8,128)(2,1)}, u32[]{:S(2)}, u32[]{:S(2)}) collective-permute-start(bf16[2048,128]{1,0:T(8,128)(2,1)S(1)} %broadcast_select_fusion), channel_id=1, source_target_pairs={{0,1},{1,0},{2,3},{3,2},{4,5},{5,4},{6,7},{7,6},{8,9},{9,8},{10,11... | collective-permute-start | bytes 1572872 | tf_op jit(solution)/shard_map/ppermute | solution.py:438
  66.4 5.9 %collective-permute-start.1 = (bf16[2048,128]{1,0:T(8,128)(2,1)}, bf16[2048,128]{1,0:T(8,128)(2,1)}, u32[]{:S(2)}, u32[]{:S(2)}) collective-permute-start(bf16[2048,128]{1,0:T(8,128)(2,1)} %collective-permute-done.first), channel_id=1, source_target_pairs={{0,16},{16,0},{32,48},{48,32},{64,80},{80,64},{96,112},{112,96},{1... | collective-permute-start | bytes 1572872 | tf_op jit(solution)/shard_map/ppermute | solution.py:439
  77.8 31.9 %copy-start.4 = (bf16[8,128]{1,0:T(8,128)(2,1)S(1)}, bf16[8,128]{1,0:T(8,128)(2,1)}, u32[]{:S(2)}) copy-start(bf16[8,128]{1,0:T(8,128)(2,1)} %query.1) | copy-start | bytes 6148
  77.8 54.5 %copy-start.5 = (f32[128]{0:T(128)S(1)}, f32[128]{0:T(128)}, u32[]{:S(2)}) copy-start(f32[128]{0:T(128)} %param.17) | copy-start | bytes 1540
  77.8 6.6 %collective-permute-start.2 = (f32[128,256]{1,0:T(8,128)S(1)}, f32[128,256]{1,0:T(8,128)S(1)}, u32[]{:S(2)}, u32[]{:S(2)}) collective-permute-start(f32[128,256]{1,0:T(8,128)S(1)} %shard_map.108), channel_id=1, source_target_pairs={{0,1},{1,0},{2,3},{3,2},{4,5},{5,4},{6,7},{7,6},{8,9},{9,8},{10,11... | collective-permute-start | bytes 393224 | tf_op jit(solution)/shard_map/ppermute | solution.py:451
  84.6 13.0 %collective-permute-start.3 = (bf16[144,256]{1,0:T(8,128)(2,1)S(1)}, bf16[144,256]{1,0:T(8,128)(2,1)S(1)}, u32[]{:S(2)}, u32[]{:S(2)}) collective-permute-start(bf16[144,256]{1,0:T(8,128)(2,1)S(1)} %shard_map.109), channel_id=1, source_target_pairs={{0,320},{16,384},{32,448},{48,0},{64,64},{80,128},{96,192},{112,25... | collective-permute-start | bytes 221192 | tf_op jit(solution)/shard_map/ppermute | solution.py:460
  97.6 3.1 %collective-permute-start.4 = (bf16[144,256]{1,0:T(8,128)(2,1)S(1)}, bf16[144,256]{1,0:T(8,128)(2,1)S(1)}, u32[]{:S(2)}, u32[]{:S(2)}) collective-permute-start(bf16[144,256]{1,0:T(8,128)(2,1)S(1)} %collective-permute-done.3.mine), channel_id=1, source_target_pairs={{0,16},{16,0},{32,48},{48,32},{64,80},{80,64},{96,112},{112,96},{1... | collective-permute-start | bytes 221192 | tf_op jit(solution)/shard_map/ppermute | solution.py:461
  101.0 8.8 %collective-permute-start.5 = (f32[128,128]{1,0:T(8,128)S(1)}, f32[128,128]{1,0:T(8,128)S(1)}, u32[]{:S(2)}, u32[]{:S(2)}) collective-permute-start(f32[128,128]{1,0:T(8,128)S(1)} %get-tuple-element.7), channel_id=1, source_target_pairs={{0,32},{16,48},{32,0},{48,16},{64,96},{80,112},{96,64},{112,80},{1... | collective-permute-start | bytes 196616 | tf_op jit(solution)/shard_map/ppermute | solution.py:463
